TPU v7x, 32 devices: a whole 2x2x4 slice. The times are simulated.
32 devices in a mesh: pp: 4 (over z), fs: 2 (over y), tp: 4 (over x, core).
Axes of the slice: x: 2, y: 2, z: 4, core: 2. Of those that a mesh axis runs over, the one named last changes fastest.
Arguments:
- tokens_in: bfloat16 [4, 8, 8, 2048], P('pp', ('fs', 'tp')), may hold values from -6 to 6
- weight_in: bfloat16 [4, 2048, 512], P('pp'), may hold values from -0.125 to 0.125
- conv_taps: float32 [4, 4, 512], P('pp'), may hold values from -3 to 3
- conv_bias: float32 [4, 512], P('pp'), may hold values from -2 to 2
- gate_rate: bfloat16 [4, 8, 64, 64], P('pp'), may hold values from -0.75 to 0.75
- bias_rate: float32 [4, 512], P('pp'), may hold values from -3 to 3
- gate_input: bfloat16 [4, 8, 64, 64], P('pp'), may hold values from -0.75 to 0.75
- bias_input: float32 [4, 512], P('pp'), may hold values from -3 to 3
- decay_param: float32 [4, 512], P('pp'), may hold values from 3.5 to 7.5
- weight_out: bfloat16 [4, 512, 2048], P('pp'), may hold values from -0.5 to 0.5
- norm_gain: float32 [4, 2048], P('pp'), may hold values from 0.1 to 1.9
- norm_shift: float32 [4, 2048], P('pp'), may hold values from -2 to 2
Outputs:
- tokens_out: bfloat16 [4, 8, 8, 2048], P('pp', ('fs', 'tp'))
All inputs are finite; a program needn't handle non-finite values.
Results may differ from a plain program's by a relative error of at most 0.022.
Values may be sent and summed in bfloat16 or wider, within the bound.
A program may use at most 128 MiB of HBM per device.

v0:
```python
import functools

import jax
import jax.numpy as jnp
from jax import lax
from jax.experimental import pallas as pl
from jax.experimental.pallas import tpu as pltpu
from jax.sharding import PartitionSpec as P

decay_scale = 8.0
norm_eps = 1e-05
mxu_width = 256
stream_parts = 4
MESH = pl.DeviceIdType.MESH


def stack_kernel(
    sections,
    tokens_hbm,
    w_in_hbm,
    taps_hbm,
    cbias_hbm,
    grate_hbm,
    brate_hbm,
    ginput_hbm,
    binput_hbm,
    dparam_hbm,
    w_out_hbm,
    gain_hbm,
    shift_hbm,
    out_ref,
    w_in,
    w_out,
    taps,
    cbias,
    grate,
    brate,
    ginput,
    binput,
    dparam,
    gain,
    shift,
    rate_map,
    input_map,
    mine,
    inbox,
    outbox,
    load_sem,
    entry_sem,
    send_sem,
    recv_sem,
    part_sem,
    final_sem,
):
    section = lax.axis_index("pp")
    column = lax.axis_index("tp")
    last = sections - 1
    pair, length = inbox.shape[1:3]
    width, lru_width = w_in.shape
    parts = part_sem.shape[1]
    core = lax.rem(column, pair)
    lead = pair - 1
    leads = core == lead
    first_stop = leads & (section == 0)
    last_stop = leads & (section == last)

    def at(stop, core_index):
        return {"pp": stop, "tp": column - core + core_index}

    barrier = pltpu.get_barrier_semaphore()

    def tell(stop, core_index):
        pl.semaphore_signal(
            barrier, inc=1, device_id=at(stop, core_index), device_id_type=MESH
        )

    @pl.when(first_stop)
    def _():
        for core_index in range(pair):
            for stop in range(sections):
                if (stop, core_index) != (0, lead):
                    tell(stop, core_index)

    @pl.when(jnp.logical_not(first_stop | last_stop))
    def _():
        tell(last, lead)

    @pl.when(leads & (section > 0))
    def _():
        @pl.when(section - 1 < last)
        def _():
            tell(section - 1, lead)

    heard = jnp.where(
        last_stop, sections * pair - 1, jnp.where(leads & (section > 0), 2, 1)
    ).astype(jnp.int32)

    def load(src, dst, index):
        return pltpu.make_async_copy(src, dst, load_sem.at[index])

    own = load(tokens_hbm.at[0, 0], mine, 0)
    load_in = load(w_in_hbm.at[0], w_in, 1)
    load_out = load(w_out_hbm.at[0], w_out, 2)
    small = [
        load(grate_hbm.at[0], grate, 3),
        load(ginput_hbm.at[0], ginput, 4),
        load(taps_hbm.at[0], taps, 5),
        load(cbias_hbm, cbias, 6),
        load(brate_hbm, brate, 7),
        load(binput_hbm, binput, 8),
        load(dparam_hbm, dparam, 9),
        load(gain_hbm, gain, 10),
        load(shift_hbm, shift, 11),
    ]
    own.start()

    @pl.when(leads)
    def _():
        for copy in small:
            copy.start()
        load_in.start()
        load_out.start()

    own.wait()
    entry = pltpu.make_async_remote_copy(
        src_ref=mine,
        dst_ref=inbox.at[section, core],
        send_sem=entry_sem,
        recv_sem=recv_sem.at[section, core],
        device_id=at(0, lead),
        device_id_type=MESH,
    )

    @pl.when(jnp.logical_not(first_stop))
    def _():
        pl.semaphore_wait(barrier, heard)
        entry.start()

    def entered(slot, core_index):
        return pltpu.make_async_remote_copy(
            src_ref=mine,
            dst_ref=inbox.at[slot, core_index],
            send_sem=entry_sem,
            recv_sem=recv_sem.at[slot, core_index],
            device_id=at(0, lead),
            device_id_type=MESH,
        )

    def onward(slot, part):
        across = slice(part * width // parts, (part + 1) * width // parts)
        return pltpu.make_async_remote_copy(
            src_ref=outbox.at[slot, :, :, across],
            dst_ref=inbox.at[slot, :, :, across],
            send_sem=send_sem.at[slot, part],
            recv_sem=part_sem.at[slot, part],
            device_id=at(jnp.minimum(section + 1, last), lead),
            device_id_type=MESH,
        )

    def home(slot, core_index):
        return pltpu.make_async_remote_copy(
            src_ref=outbox.at[slot, core_index],
            dst_ref=out_ref.at[0, 0],
            send_sem=send_sem.at[slot, core_index],
            recv_sem=final_sem,
            device_id=at(slot, core_index),
            device_id_type=MESH,
        )

    def run_section():
        blocks, block_width, _ = grate.shape
        group = max(1, min(blocks, mxu_width // block_width))
        wide = group * block_width
        rate_map[...] = jnp.zeros_like(rate_map)
        input_map[...] = jnp.zeros_like(input_map)
        for copy in small:
            copy.wait()
        for block in range(blocks):
            to = (block % group) * block_width
            rate_map[block // group, to : to + block_width, to : to + block_width] = grate[block]
            input_map[block // group, to : to + block_width, to : to + block_width] = ginput[block]
        minus_decay = -dparam[...]
        softplus = jnp.maximum(minus_decay, 0.0) + jnp.log1p(jnp.exp(-jnp.abs(minus_decay)))
        dparam[...] = -decay_scale * softplus
        load_in.wait()
        load_out.wait()

        @pl.when(section == 0)
        def _():
            inbox[0, lead] = mine[...]

        position = lax.broadcasted_iota(jnp.int32, (pair, length, lru_width), 1)

        def delayed(x, by, fill):
            return jnp.where(position >= by, pltpu.roll(x, by, 1), fill)

        def one_slot(slot, carry):
            @pl.when(section == 0)
            def _():
                for core_index in range(pair):
                    if core_index == lead:
                        @pl.when(slot > 0)
                        def _():
                            entered(slot, core_index).wait_recv()
                    else:
                        entered(slot, core_index).wait_recv()

            rows = pair * length
            projected = jnp.zeros((rows, lru_width), jnp.float32)
            streams = []
            for part in range(parts):
                @pl.when(section > 0)
                def _():
                    onward(slot, part).wait_recv()

                across = slice(part * width // parts, (part + 1) * width // parts)
                piece = inbox[slot, :, :, across].astype(jnp.float32).reshape(rows, -1)
                streams.append(piece)
                projected = projected + jnp.dot(
                    piece.astype(jnp.bfloat16),
                    w_in[across, :],
                    preferred_element_type=jnp.float32,
                )
            stream = jnp.concatenate(streams, axis=1)
            projected = projected.astype(jnp.bfloat16).astype(jnp.float32)
            projected = projected.reshape(pair, length, lru_width)
            tap_count = taps.shape[0]
            convolved = cbias[...][None]
            for tap in range(tap_count):
                by = tap_count - 1 - tap
                shifted = delayed(projected, by, 0.0) if by else projected
                convolved = convolved + shifted * taps[tap : tap + 1][None]
            convolved = convolved.reshape(rows, lru_width).astype(jnp.bfloat16)

            def mapped(maps):
                return jnp.concatenate(
                    [
                        jnp.dot(
                            convolved[:, i * wide : (i + 1) * wide],
                            maps[i],
                            preferred_element_type=jnp.float32,
                        )
                        for i in range(blocks // group)
                    ],
                    axis=1,
                )

            rate_gate = jax.nn.sigmoid(mapped(rate_map) + brate[...])
            input_gate = jax.nn.sigmoid(mapped(input_map) + binput[...])
            log_decay = rate_gate * dparam[...]
            decay = jnp.exp(log_decay)
            scale_in = jnp.sqrt(-jnp.tanh(log_decay) * (decay * decay + 1.0))
            hidden = scale_in * input_gate * convolved.astype(jnp.float32)
            hidden = hidden.reshape(pair, length, lru_width)
            decay = decay.reshape(pair, length, lru_width)
            by = 1
            while by < length:
                hidden = decay * delayed(hidden, by, 0.0) + hidden
                if 2 * by < length:
                    decay = decay * delayed(decay, by, 1.0)
                by *= 2
            mixed = hidden.reshape(rows, lru_width).astype(jnp.bfloat16)
            summed = stream + jnp.dot(mixed, w_out[...], preferred_element_type=jnp.float32)
            away = summed - jnp.mean(stream, axis=-1, keepdims=True)
            offset = jnp.mean(away, axis=-1, keepdims=True)
            square = jnp.mean(away * away, axis=-1, keepdims=True)
            variance = jnp.maximum(square - offset * offset, 0.0)
            normed = (away - offset) * lax.rsqrt(variance + norm_eps) * gain[...] + shift[...]
            outbox[slot] = normed.reshape(pair, length, -1).astype(jnp.bfloat16)

            @pl.when((section == 0) & (slot == 0))
            def _():
                pl.semaphore_wait(barrier, heard)

            @pl.when(section < last)
            def _():
                for part in range(parts):
                    onward(slot, part).start()

            @pl.when(section == last)
            def _():
                for core_index in range(pair):
                    if core_index == lead:
                        @pl.when(slot < last)
                        def _():
                            home(slot, core_index).start()

                        @pl.when(slot == last)
                        def _():
                            out_ref[0, 0] = outbox[slot, core_index]
                    else:
                        home(slot, core_index).start()

            return carry

        lax.fori_loop(0, sections, one_slot, 0)

        @pl.when(section < last)
        def _():
            def sent(slot, carry):
                for part in range(parts):
                    onward(slot, part).wait_send()
                return carry

            lax.fori_loop(0, sections, sent, 0)

        @pl.when(section == last)
        def _():
            def sent(slot, carry):
                for core_index in range(pair):
                    if core_index == lead:
                        @pl.when(slot < last)
                        def _():
                            home(slot, core_index).wait_send()
                    else:
                        home(slot, core_index).wait_send()
                return carry

            lax.fori_loop(0, sections, sent, 0)

    pl.when(leads)(run_section)

    @pl.when(jnp.logical_not(first_stop))
    def _():
        entry.wait_send()

    @pl.when(jnp.logical_not(last_stop))
    def _():
        home(0, 0).wait_recv()


def shards(sections, pair, tokens_in, *weights):
    _, _, length, width = tokens_in.shape
    lru_width = weights[0].shape[2]
    tap_count = weights[1].shape[1]
    _, blocks, block_width, _ = weights[3].shape
    group = max(1, min(blocks, mxu_width // block_width))
    wide = group * block_width
    vmem = pltpu.VMEM
    f32, bf16 = jnp.float32, jnp.bfloat16
    return pl.pallas_call(
        functools.partial(stack_kernel, sections),
        out_shape=pltpu.VMEM(tokens_in.shape, tokens_in.dtype),
        in_specs=[pl.BlockSpec(memory_space=pl.ANY)] * (1 + len(weights)),
        out_specs=pl.BlockSpec(memory_space=pltpu.VMEM),
        scratch_shapes=[
            vmem((width, lru_width), bf16),
            vmem((lru_width, width), bf16),
            vmem((tap_count, lru_width), f32),
            vmem((1, lru_width), f32),
            vmem((blocks, block_width, block_width), bf16),
            vmem((1, lru_width), f32),
            vmem((blocks, block_width, block_width), bf16),
            vmem((1, lru_width), f32),
            vmem((1, lru_width), f32),
            vmem((1, width), f32),
            vmem((1, width), f32),
            vmem((blocks // group, wide, wide), bf16),
            vmem((blocks // group, wide, wide), bf16),
            vmem((length, width), bf16),
            vmem((sections, pair, length, width), bf16),
            vmem((sections, pair, length, width), bf16),
            pltpu.SemaphoreType.DMA((12,)),
            pltpu.SemaphoreType.DMA,
            pltpu.SemaphoreType.DMA((sections, max(pair, stream_parts))),
            pltpu.SemaphoreType.DMA((sections, pair)),
            pltpu.SemaphoreType.DMA((sections, stream_parts)),
            pltpu.SemaphoreType.DMA,
        ],
        compiler_params=pltpu.CompilerParams(collective_id=0, has_side_effects=True),
        name="section_stack",
    )(tokens_in, *weights)


def solution(mesh):
    placed = (
        P("pp", ("fs", "tp"), None, None),
        P("pp", None, None),
        P("pp", None, None),
        P("pp", None),
        P("pp", None, None, None),
        P("pp", None),
        P("pp", None, None, None),
        P("pp", None),
        P("pp", None),
        P("pp", None, None),
        P("pp", None),
        P("pp", None),
    )
    pair = 2 if mesh.shape["tp"] % 2 == 0 else 1
    return jax.shard_map(
        functools.partial(shards, mesh.shape["pp"], pair),
        mesh=mesh,
        in_specs=placed,
        out_specs=P("pp", ("fs", "tp"), None, None),
        check_vma=False,
    )
```

profile of v0, /device:TPU:17, one launch (start us, length us, event | category | flops | bytes accessed | tf_op | source)
XLA Modules:
  0.0 18.7 jit_solution(7183893981690263204)
XLA Ops:
  0.0 18.1 %section_stack.1 = bf16[1,1,8,2048]{3,2,1,0:T(8,128)(2,1)S(1)} custom-call(bf16[1,1,8,2048]{3,2,1,0:T(8,128)(2,1)} %tokens_hbm.1, bf16[1,2048,512]{2,1,0:T(8,128)(2,1)} %w_in_hbm.1, f32[1,4,512]{2,1,0:T(4,128)} %taps_hbm.1, f32[1,512]{1,0:T(1,128)} %cbias_hbm.1, bf16[1,8,64,64]{3,2,1,0:T(8,128)(2,1)} %grate_hbm.1, f32[1,512]{1,0:T(1,128)} %brate_hbm.1, ...), custom_call_target="tpu_custom_call" | custom-call | tf_op jit(solution)/shard_map/section_stack/pallas_call | solution.py:341
  18.1 0.6 %copy.14 = bf16[1,1,8,2048]{3,2,1,0:T(8,128)(2,1)} copy(bf16[1,1,8,2048]{3,2,1,0:T(8,128)(2,1)S(1)} %section_stack.1) | data formatting | bytes 65536
where the time goes:
time: 18.9 us; the launch traced here: 18.7 us
  Pallas kernels  18.1 us (96%)
  local copies, waits for them, and re-layouts  0.62 us (3%)
    pallas_call x1, Pallas kernels, shards(): pl.pallas_call(functools.partial(stack_kernel, sections), out_shape=pltpu...  18.1 us
    unnamed x1, local copies, waits for them, and re-layouts  0.62 us

commit v1 on v0

--- a/solution.py
+++ b/solution.py
@@ -49,15 +49,15 @@
     entry_sem,
     send_sem,
     recv_sem,
-    part_sem,
     final_sem,
+    ready_sem,
 ):
     section = lax.axis_index("pp")
     column = lax.axis_index("tp")
     last = sections - 1
     pair, length = inbox.shape[1:3]
     width, lru_width = w_in.shape
-    parts = part_sem.shape[1]
+    parts = recv_sem.shape[1]
     core = lax.rem(column, pair)
     lead = pair - 1
     leads = core == lead
@@ -67,6 +67,9 @@
     def at(stop, core_index):
         return {"pp": stop, "tp": column - core + core_index}
 
+    def across(part):
+        return slice(part * width // parts, (part + 1) * width // parts)
+
     barrier = pltpu.get_barrier_semaphore()
 
     def tell(stop, core_index):
@@ -74,10 +77,32 @@
             barrier, inc=1, device_id=at(stop, core_index), device_id_type=MESH
         )
 
+    def load(src, dst, index):
+        return pltpu.make_async_copy(src, dst, load_sem.at[index])
+
+    own = load(tokens_hbm.at[0, 0], mine, 0)
+    small = [
+        load(grate_hbm.at[0], grate, 1),
+        load(ginput_hbm.at[0], ginput, 2),
+        load(taps_hbm.at[0], taps, 3),
+        load(cbias_hbm, cbias, 4),
+        load(brate_hbm, brate, 5),
+        load(binput_hbm, binput, 6),
+        load(dparam_hbm, dparam, 7),
+        load(gain_hbm, gain, 8),
+        load(shift_hbm, shift, 9),
+    ]
+    load_out = load(w_out_hbm.at[0], w_out, 10)
+    load_in = [
+        load(w_in_hbm.at[0, across(part)], w_in.at[across(part)], 11 + part)
+        for part in range(parts)
+    ]
+    own.start()
+
     @pl.when(first_stop)
     def _():
-        for core_index in range(pair):
-            for stop in range(sections):
+        for stop in reversed(range(sections)):
+            for core_index in range(pair):
                 if (stop, core_index) != (0, lead):
                     tell(stop, core_index)
 
@@ -85,74 +110,72 @@
     def _():
         tell(last, lead)
 
-    @pl.when(leads & (section > 0))
-    def _():
-        @pl.when(section - 1 < last)
-        def _():
-            tell(section - 1, lead)
+    @pl.when(leads & (section > 0) & (section + 1 < last))
+    def _():
+        tell(section + 1, lead)
 
     heard = jnp.where(
-        last_stop, sections * pair - 1, jnp.where(leads & (section > 0), 2, 1)
+        last_stop, sections * pair - 1, jnp.where(leads & (section > 1), 2, 1)
     ).astype(jnp.int32)
-
-    def load(src, dst, index):
-        return pltpu.make_async_copy(src, dst, load_sem.at[index])
-
-    own = load(tokens_hbm.at[0, 0], mine, 0)
-    load_in = load(w_in_hbm.at[0], w_in, 1)
-    load_out = load(w_out_hbm.at[0], w_out, 2)
-    small = [
-        load(grate_hbm.at[0], grate, 3),
-        load(ginput_hbm.at[0], ginput, 4),
-        load(taps_hbm.at[0], taps, 5),
-        load(cbias_hbm, cbias, 6),
-        load(brate_hbm, brate, 7),
-        load(binput_hbm, binput, 8),
-        load(dparam_hbm, dparam, 9),
-        load(gain_hbm, gain, 10),
-        load(shift_hbm, shift, 11),
-    ]
-    own.start()
 
     @pl.when(leads)
     def _():
         for copy in small:
             copy.start()
-        load_in.start()
+        for copy in load_in:
+            copy.start()
         load_out.start()
 
     own.wait()
-    entry = pltpu.make_async_remote_copy(
-        src_ref=mine,
-        dst_ref=inbox.at[section, core],
-        send_sem=entry_sem,
-        recv_sem=recv_sem.at[section, core],
-        device_id=at(0, lead),
-        device_id_type=MESH,
-    )
+
+    def entry(part):
+        return pltpu.make_async_remote_copy(
+            src_ref=mine.at[:, across(part)],
+            dst_ref=inbox.at[section, core, :, across(part)],
+            send_sem=entry_sem,
+            recv_sem=recv_sem.at[section, part],
+            device_id=at(0, lead),
+            device_id_type=MESH,
+        )
 
     @pl.when(jnp.logical_not(first_stop))
     def _():
         pl.semaphore_wait(barrier, heard)
-        entry.start()
-
-    def entered(slot, core_index):
-        return pltpu.make_async_remote_copy(
-            src_ref=mine,
-            dst_ref=inbox.at[slot, core_index],
+        for part in range(parts):
+            entry(part).start()
+
+    @pl.when(leads & (section > 0))
+    def _():
+        pl.semaphore_signal(
+            ready_sem, inc=1, device_id=at(section - 1, lead), device_id_type=MESH
+        )
+
+    def arrival(slot, part, cores):
+        return pltpu.make_async_remote_copy(
+            src_ref=outbox.at[slot, cores, :, across(part)],
+            dst_ref=inbox.at[slot, cores, :, across(part)],
             send_sem=entry_sem,
-            recv_sem=recv_sem.at[slot, core_index],
+            recv_sem=recv_sem.at[slot, part],
             device_id=at(0, lead),
             device_id_type=MESH,
         )
 
     def onward(slot, part):
-        across = slice(part * width // parts, (part + 1) * width // parts)
-        return pltpu.make_async_remote_copy(
-            src_ref=outbox.at[slot, :, :, across],
-            dst_ref=inbox.at[slot, :, :, across],
-            send_sem=send_sem.at[slot, part],
-            recv_sem=part_sem.at[slot, part],
+        return pltpu.make_async_remote_copy(
+            src_ref=outbox.at[slot, :, :, across(part)],
+            dst_ref=inbox.at[slot, :, :, across(part)],
+            send_sem=send_sem.at[slot],
+            recv_sem=recv_sem.at[slot, part],
+            device_id=at(jnp.minimum(section + 1, last), lead),
+            device_id_type=MESH,
+        )
+
+    def onward_all(slot):
+        return pltpu.make_async_remote_copy(
+            src_ref=outbox.at[slot],
+            dst_ref=inbox.at[slot],
+            send_sem=send_sem.at[slot],
+            recv_sem=recv_sem.at[slot, 0],
             device_id=at(jnp.minimum(section + 1, last), lead),
             device_id_type=MESH,
         )
@@ -161,9 +184,19 @@
         return pltpu.make_async_remote_copy(
             src_ref=outbox.at[slot, core_index],
             dst_ref=out_ref.at[0, 0],
-            send_sem=send_sem.at[slot, core_index],
+            send_sem=send_sem.at[slot],
             recv_sem=final_sem,
             device_id=at(slot, core_index),
+            device_id_type=MESH,
+        )
+
+    def homes_sent(slot, cores):
+        return pltpu.make_async_remote_copy(
+            src_ref=outbox.at[slot, cores],
+            dst_ref=inbox.at[slot, cores],
+            send_sem=send_sem.at[slot],
+            recv_sem=final_sem,
+            device_id=at(slot, lead),
             device_id_type=MESH,
         )
 
@@ -182,8 +215,6 @@
         minus_decay = -dparam[...]
         softplus = jnp.maximum(minus_decay, 0.0) + jnp.log1p(jnp.exp(-jnp.abs(minus_decay)))
         dparam[...] = -decay_scale * softplus
-        load_in.wait()
-        load_out.wait()
 
         @pl.when(section == 0)
         def _():
@@ -195,30 +226,29 @@
             return jnp.where(position >= by, pltpu.roll(x, by, 1), fill)
 
         def one_slot(slot, carry):
-            @pl.when(section == 0)
-            def _():
-                for core_index in range(pair):
-                    if core_index == lead:
-                        @pl.when(slot > 0)
-                        def _():
-                            entered(slot, core_index).wait_recv()
-                    else:
-                        entered(slot, core_index).wait_recv()
-
             rows = pair * length
             projected = jnp.zeros((rows, lru_width), jnp.float32)
             streams = []
+            entering = (section == 0) & (slot == 0)
             for part in range(parts):
-                @pl.when(section > 0)
+                @pl.when(slot == 0)
                 def _():
-                    onward(slot, part).wait_recv()
-
-                across = slice(part * width // parts, (part + 1) * width // parts)
-                piece = inbox[slot, :, :, across].astype(jnp.float32).reshape(rows, -1)
+                    load_in[part].wait()
+
+                @pl.when(jnp.logical_not(entering))
+                def _():
+                    arrival(slot, part, slice(0, pair)).wait_recv()
+
+                if lead:
+                    @pl.when(entering)
+                    def _():
+                        arrival(slot, part, slice(0, lead)).wait_recv()
+
+                piece = inbox[slot, :, :, across(part)].astype(jnp.float32).reshape(rows, -1)
                 streams.append(piece)
                 projected = projected + jnp.dot(
                     piece.astype(jnp.bfloat16),
-                    w_in[across, :],
+                    w_in[across(part), :],
                     preferred_element_type=jnp.float32,
                 )
             stream = jnp.concatenate(streams, axis=1)
@@ -259,6 +289,10 @@
                 if 2 * by < length:
                     decay = decay * delayed(decay, by, 1.0)
                 by *= 2
+            @pl.when(slot == 0)
+            def _():
+                load_out.wait()
+
             mixed = hidden.reshape(rows, lru_width).astype(jnp.bfloat16)
             summed = stream + jnp.dot(mixed, w_out[...], preferred_element_type=jnp.float32)
             away = summed - jnp.mean(stream, axis=-1, keepdims=True)
@@ -268,9 +302,9 @@
             normed = (away - offset) * lax.rsqrt(variance + norm_eps) * gain[...] + shift[...]
             outbox[slot] = normed.reshape(pair, length, -1).astype(jnp.bfloat16)
 
-            @pl.when((section == 0) & (slot == 0))
+            @pl.when((section < last) & (slot == 0))
             def _():
-                pl.semaphore_wait(barrier, heard)
+                pl.semaphore_wait(ready_sem, 1)
 
             @pl.when(section < last)
             def _():
@@ -297,32 +331,28 @@
 
         @pl.when(section < last)
         def _():
-            def sent(slot, carry):
-                for part in range(parts):
-                    onward(slot, part).wait_send()
-                return carry
-
-            lax.fori_loop(0, sections, sent, 0)
+            for slot in range(sections):
+                onward_all(slot).wait_send()
 
         @pl.when(section == last)
         def _():
-            def sent(slot, carry):
-                for core_index in range(pair):
-                    if core_index == lead:
-                        @pl.when(slot < last)
-                        def _():
-                            home(slot, core_index).wait_send()
-                    else:
-                        home(slot, core_index).wait_send()
-                return carry
-
-            lax.fori_loop(0, sections, sent, 0)
+            for slot in range(last):
+                homes_sent(slot, slice(0, pair)).wait_send()
+            if lead:
+                homes_sent(last, slice(0, lead)).wait_send()
 
     pl.when(leads)(run_section)
 
     @pl.when(jnp.logical_not(first_stop))
     def _():
-        entry.wait_send()
+        pltpu.make_async_remote_copy(
+            src_ref=mine,
+            dst_ref=inbox.at[section, core],
+            send_sem=entry_sem,
+            recv_sem=recv_sem.at[section, 0],
+            device_id=at(0, lead),
+            device_id_type=MESH,
+        ).wait_send()
 
     @pl.when(jnp.logical_not(last_stop))
     def _():
@@ -360,12 +390,12 @@
             vmem((length, width), bf16),
             vmem((sections, pair, length, width), bf16),
             vmem((sections, pair, length, width), bf16),
-            pltpu.SemaphoreType.DMA((12,)),
+            pltpu.SemaphoreType.DMA((11 + stream_parts,)),
             pltpu.SemaphoreType.DMA,
-            pltpu.SemaphoreType.DMA((sections, max(pair, stream_parts))),
-            pltpu.SemaphoreType.DMA((sections, pair)),
+            pltpu.SemaphoreType.DMA((sections,)),
             pltpu.SemaphoreType.DMA((sections, stream_parts)),
             pltpu.SemaphoreType.DMA,
+            pltpu.SemaphoreType.REGULAR,
         ],
         compiler_params=pltpu.CompilerParams(collective_id=0, has_side_effects=True),
         name="section_stack",

time: 18.9 us -> 18.8 us (level)
  no operation moved by 1% of the time
where the time goes in v1:
time: 18.8 us; the launch traced here: 18.6 us
  Pallas kernels  18 us (96%)
  local copies, waits for them, and re-layouts  0.62 us (3%)
    pallas_call x1, Pallas kernels, shards(): pl.pallas_call(functools.partial(stack_kernel, sections), out_shape=pltpu...  18 us
    unnamed x1, local copies, waits for them, and re-layouts  0.62 us

profile of v1, /device:TPU:17, one launch (start us, length us, event | category | flops | bytes accessed | tf_op | source)
XLA Modules:
  0.0 18.6 jit_solution(17246924817263966797)
XLA Ops:
  0.0 18.0 %section_stack.1 = bf16[1,1,8,2048]{3,2,1,0:T(8,128)(2,1)S(1)} custom-call(bf16[1,1,8,2048]{3,2,1,0:T(8,128)(2,1)} %tokens_hbm.1, bf16[1,2048,512]{2,1,0:T(8,128)(2,1)} %w_in_hbm.1, f32[1,4,512]{2,1,0:T(4,128)} %taps_hbm.1, f32[1,512]{1,0:T(1,128)} %cbias_hbm.1, bf16[1,8,64,64]{3,2,1,0:T(8,128)(2,1)} %grate_hbm.1, f32[1,512]{1,0:T(1,128)} %brate_hbm.1, ...), custom_call_target="tpu_custom_call" | custom-call | tf_op jit(solution)/shard_map/section_stack/pallas_call | solution.py:371
  18.0 0.6 %copy.14 = bf16[1,1,8,2048]{3,2,1,0:T(8,128)(2,1)} copy(bf16[1,1,8,2048]{3,2,1,0:T(8,128)(2,1)S(1)} %section_stack.1) | data formatting | bytes 65536

commit v2 on v1

--- a/solution.py
+++ b/solution.py
@@ -10,8 +10,16 @@
 decay_scale = 8.0
 norm_eps = 1e-05
 mxu_width = 256
-stream_parts = 4
+mxus = 2
+lanes = 128
 MESH = pl.DeviceIdType.MESH
+
+
+def fold_lanes(x):
+    total = x[:, :lanes]
+    for start in range(lanes, x.shape[1], lanes):
+        total = total + x[:, start : start + lanes]
+    return total
 
 
 def stack_kernel(
@@ -32,16 +40,13 @@
     w_in,
     w_out,
     taps,
-    cbias,
-    grate,
-    brate,
-    ginput,
-    binput,
-    dparam,
-    gain,
-    shift,
-    rate_map,
-    input_map,
+    channel,
+    gates,
+    norm,
+    before,
+    maps,
+    folded,
+    base,
     mine,
     inbox,
     outbox,
@@ -50,14 +55,18 @@
     send_sem,
     recv_sem,
     final_sem,
+    norm_sem,
     ready_sem,
 ):
     section = lax.axis_index("pp")
     column = lax.axis_index("tp")
     last = sections - 1
     pair, length = inbox.shape[1:3]
+    rows = pair * length
     width, lru_width = w_in.shape
     parts = recv_sem.shape[1]
+    part_width = width // parts
+    tiles_in = width // mxu_width
     core = lax.rem(column, pair)
     lead = pair - 1
     leads = core == lead
@@ -68,7 +77,7 @@
         return {"pp": stop, "tp": column - core + core_index}
 
     def across(part):
-        return slice(part * width // parts, (part + 1) * width // parts)
+        return slice(part * part_width, (part + 1) * part_width)
 
     barrier = pltpu.get_barrier_semaphore()
 
@@ -82,21 +91,18 @@
 
     own = load(tokens_hbm.at[0, 0], mine, 0)
     small = [
-        load(grate_hbm.at[0], grate, 1),
-        load(ginput_hbm.at[0], ginput, 2),
+        load(grate_hbm.at[0], gates.at[0], 1),
+        load(ginput_hbm.at[0], gates.at[1], 2),
         load(taps_hbm.at[0], taps, 3),
-        load(cbias_hbm, cbias, 4),
-        load(brate_hbm, brate, 5),
-        load(binput_hbm, binput, 6),
-        load(dparam_hbm, dparam, 7),
-        load(gain_hbm, gain, 8),
-        load(shift_hbm, shift, 9),
+        load(cbias_hbm, channel.at[0], 4),
+        load(brate_hbm, channel.at[1], 5),
+        load(binput_hbm, channel.at[2], 6),
+        load(dparam_hbm, channel.at[3], 7),
+        load(gain_hbm, norm.at[0], 8),
+        load(shift_hbm, norm.at[1], 9),
     ]
-    load_out = load(w_out_hbm.at[0], w_out, 10)
-    load_in = [
-        load(w_in_hbm.at[0, across(part)], w_in.at[across(part)], 11 + part)
-        for part in range(parts)
-    ]
+    load_in = load(w_in_hbm.at[0], w_in, 10)
+    load_out = load(w_out_hbm.at[0], w_out, 11)
     own.start()
 
     @pl.when(first_stop)
@@ -122,9 +128,18 @@
     def _():
         for copy in small:
             copy.start()
-        for copy in load_in:
-            copy.start()
+        load_in.start()
         load_out.start()
+
+    @pl.when(jnp.logical_not(first_stop))
+    def _():
+        pl.semaphore_wait(barrier, heard)
+
+    @pl.when(leads & (section > 0))
+    def _():
+        pl.semaphore_signal(
+            ready_sem, inc=1, device_id=at(section - 1, lead), device_id_type=MESH
+        )
 
     own.wait()
 
@@ -140,15 +155,8 @@
 
     @pl.when(jnp.logical_not(first_stop))
     def _():
-        pl.semaphore_wait(barrier, heard)
         for part in range(parts):
             entry(part).start()
-
-    @pl.when(leads & (section > 0))
-    def _():
-        pl.semaphore_signal(
-            ready_sem, inc=1, device_id=at(section - 1, lead), device_id_type=MESH
-        )
 
     def arrival(slot, part, cores):
         return pltpu.make_async_remote_copy(
@@ -200,41 +208,121 @@
             device_id_type=MESH,
         )
 
-    def run_section():
-        blocks, block_width, _ = grate.shape
-        group = max(1, min(blocks, mxu_width // block_width))
-        wide = group * block_width
-        rate_map[...] = jnp.zeros_like(rate_map)
-        input_map[...] = jnp.zeros_like(input_map)
+    norm_onward = pltpu.make_async_remote_copy(
+        src_ref=norm,
+        dst_ref=before,
+        send_sem=norm_sem.at[0],
+        recv_sem=norm_sem.at[1],
+        device_id=at(jnp.minimum(section + 1, last), lead),
+        device_id_type=MESH,
+    )
+
+    def tile(ref, row, col):
+        return ref[
+            row * mxu_width : (row + 1) * mxu_width,
+            col * mxu_width : (col + 1) * mxu_width,
+        ]
+
+    def unit(index, mxu):
+        index = index % (tiles_in + 2 + mxus * parts)
+        if index < tiles_in:
+            return tile(w_in, index, mxu)
+        index -= tiles_in
+        if index < 2:
+            return maps[index, mxu]
+        index -= 2
+        return tile(w_out, index % mxus, (index // mxus) * mxus + mxu)
+
+    def stage(index, mxu):
+        pltpu.matmul_push_rhs(unit(index, mxu), staging_register=index % 2, mxu_index=mxu)
+
+    def step(index, accs, lhs):
+        for mxu in range(mxus):
+            pltpu.matmul_acc_lhs(accs[mxu], lhs[mxu], load_staged_rhs=index % 2)
+        for mxu in range(mxus):
+            stage(index + 2, mxu)
+
+    def popped(accs):
+        return jnp.concatenate([pltpu.matmul_pop(acc) for acc in accs], axis=1)
+
+    def run_section(acc_in, acc_rate, acc_input, acc_out):
+        def drain():
+            nothing = jnp.zeros((rows, mxu_width), jnp.bfloat16)
+            for mxu in range(mxus):
+                for register in range(2):
+                    pltpu.matmul_acc_lhs(acc_in[mxu], nothing, load_staged_rhs=register)
+            popped(acc_in)
+
+        drain()
+        for accs in (acc_rate, acc_input, *acc_out):
+            popped(accs)
+        _, blocks, block_width, _ = gates.shape
+        group = mxu_width // block_width
+        maps[...] = jnp.zeros_like(maps)
         for copy in small:
             copy.wait()
-        for block in range(blocks):
-            to = (block % group) * block_width
-            rate_map[block // group, to : to + block_width, to : to + block_width] = grate[block]
-            input_map[block // group, to : to + block_width, to : to + block_width] = ginput[block]
-        minus_decay = -dparam[...]
+
+        @pl.when(section < last)
+        def _():
+            pl.semaphore_wait(ready_sem, 1)
+            norm_onward.start()
+
+        for gate in range(2):
+            for block in range(blocks):
+                to = (block % group) * block_width
+                maps[gate, block // group, to : to + block_width, to : to + block_width] = gates[
+                    gate, block
+                ]
+        minus_decay = -channel[3]
         softplus = jnp.maximum(minus_decay, 0.0) + jnp.log1p(jnp.exp(-jnp.abs(minus_decay)))
-        dparam[...] = -decay_scale * softplus
+        channel[3] = -decay_scale * softplus
+        load_in.wait()
 
         @pl.when(section == 0)
         def _():
             inbox[0, lead] = mine[...]
-
+            before[0] = jnp.ones_like(before[0])
+            before[1] = jnp.zeros_like(before[1])
+            folded[...] = jnp.zeros_like(folded)
+
+        @pl.when(section > 0)
+        def _():
+            norm_onward.wait_recv()
+            which = lax.broadcasted_iota(jnp.int32, (rows, mxu_width), 0)
+            for k in range(tiles_in):
+                cols = slice(k * mxu_width, (k + 1) * mxu_width)
+                split = []
+                for vector in range(2):
+                    value = before[vector, :, cols]
+                    high = value.astype(jnp.bfloat16).astype(jnp.float32)
+                    split += [high, value - high]
+                lhs = jnp.zeros((rows, mxu_width), jnp.float32)
+                for row, value in enumerate(split):
+                    lhs = jnp.where(which == row, value, lhs)
+                lhs = lhs.astype(jnp.bfloat16)
+                for mxu in range(mxus):
+                    stage(k, mxu)
+                    pltpu.matmul_acc_lhs(acc_in[mxu], lhs, load_staged_rhs=k % 2)
+            result = popped(acc_in)
+            folded[0] = result[0:1] + result[1:2]
+            folded[1] = result[2:3] + result[3:4]
+            before[1] = before[1] - jnp.mean(before[1])
+
+        load_out.wait()
+        for mxu in range(mxus):
+            stage(0, mxu)
+            stage(1, mxu)
         position = lax.broadcasted_iota(jnp.int32, (pair, length, lru_width), 1)
 
         def delayed(x, by, fill):
             return jnp.where(position >= by, pltpu.roll(x, by, 1), fill)
 
         def one_slot(slot, carry):
-            rows = pair * length
-            projected = jnp.zeros((rows, lru_width), jnp.float32)
-            streams = []
             entering = (section == 0) & (slot == 0)
+            total = jnp.zeros((rows, lanes), jnp.float32)
+            squares = jnp.zeros((rows, lanes), jnp.float32)
+            index = 0
             for part in range(parts):
-                @pl.when(slot == 0)
-                def _():
-                    load_in[part].wait()
-
                 @pl.when(jnp.logical_not(entering))
                 def _():
                     arrival(slot, part, slice(0, pair)).wait_recv()
@@ -244,40 +332,40 @@
                     def _():
                         arrival(slot, part, slice(0, lead)).wait_recv()
 
-                piece = inbox[slot, :, :, across(part)].astype(jnp.float32).reshape(rows, -1)
-                streams.append(piece)
-                projected = projected + jnp.dot(
-                    piece.astype(jnp.bfloat16),
-                    w_in[across(part), :],
-                    preferred_element_type=jnp.float32,
-                )
-            stream = jnp.concatenate(streams, axis=1)
+                raw = inbox[slot, :, :, across(part)].astype(jnp.float32).reshape(rows, -1)
+                total = total + fold_lanes(raw)
+                squares = squares + fold_lanes(raw * raw)
+                scaled = (raw * before[0, :, across(part)]).astype(jnp.bfloat16)
+                for start in range(0, part_width, mxu_width):
+                    lhs = scaled[:, start : start + mxu_width]
+                    step(index, acc_in, [lhs] * mxus)
+                    index += 1
+            mean = jnp.sum(total, axis=-1, keepdims=True) / width
+            square = jnp.sum(squares, axis=-1, keepdims=True) / width
+            variance = jnp.maximum(square - mean * mean, 0.0)
+            scale = jnp.where(section > 0, lax.rsqrt(variance + norm_eps), 1.0)
+            lower = scale * mean
+            projected = popped(acc_in) * scale - lower * folded[0] + folded[1]
             projected = projected.astype(jnp.bfloat16).astype(jnp.float32)
             projected = projected.reshape(pair, length, lru_width)
             tap_count = taps.shape[0]
-            convolved = cbias[...][None]
+            convolved = channel[0][None]
             for tap in range(tap_count):
                 by = tap_count - 1 - tap
                 shifted = delayed(projected, by, 0.0) if by else projected
                 convolved = convolved + shifted * taps[tap : tap + 1][None]
             convolved = convolved.reshape(rows, lru_width).astype(jnp.bfloat16)
-
-            def mapped(maps):
-                return jnp.concatenate(
-                    [
-                        jnp.dot(
-                            convolved[:, i * wide : (i + 1) * wide],
-                            maps[i],
-                            preferred_element_type=jnp.float32,
-                        )
-                        for i in range(blocks // group)
-                    ],
-                    axis=1,
-                )
-
-            rate_gate = jax.nn.sigmoid(mapped(rate_map) + brate[...])
-            input_gate = jax.nn.sigmoid(mapped(input_map) + binput[...])
-            log_decay = rate_gate * dparam[...]
+            lhs = [convolved[:, m * mxu_width : (m + 1) * mxu_width] for m in range(mxus)]
+            step(index, acc_rate, lhs)
+            step(index + 1, acc_input, lhs)
+            index += 2
+            for part in range(parts):
+                raw = inbox[slot, :, :, across(part)].astype(jnp.float32).reshape(rows, -1)
+                gain, shift = before[0, :, across(part)], before[1, :, across(part)]
+                base[:, across(part)] = (raw * scale - lower) * gain + shift
+            rate_gate = jax.nn.sigmoid(popped(acc_rate) + channel[1])
+            input_gate = jax.nn.sigmoid(popped(acc_input) + channel[2])
+            log_decay = rate_gate * channel[3]
             decay = jnp.exp(log_decay)
             scale_in = jnp.sqrt(-jnp.tanh(log_decay) * (decay * decay + 1.0))
             hidden = scale_in * input_gate * convolved.astype(jnp.float32)
@@ -289,30 +377,38 @@
                 if 2 * by < length:
                     decay = decay * delayed(decay, by, 1.0)
                 by *= 2
-            @pl.when(slot == 0)
-            def _():
-                load_out.wait()
-
             mixed = hidden.reshape(rows, lru_width).astype(jnp.bfloat16)
-            summed = stream + jnp.dot(mixed, w_out[...], preferred_element_type=jnp.float32)
-            away = summed - jnp.mean(stream, axis=-1, keepdims=True)
-            offset = jnp.mean(away, axis=-1, keepdims=True)
-            square = jnp.mean(away * away, axis=-1, keepdims=True)
-            variance = jnp.maximum(square - offset * offset, 0.0)
-            normed = (away - offset) * lax.rsqrt(variance + norm_eps) * gain[...] + shift[...]
-            outbox[slot] = normed.reshape(pair, length, -1).astype(jnp.bfloat16)
-
-            @pl.when((section < last) & (slot == 0))
-            def _():
-                pl.semaphore_wait(ready_sem, 1)
-
-            @pl.when(section < last)
-            def _():
-                for part in range(parts):
+
+            def project(part):
+                for k in range(mxus):
+                    lhs = mixed[:, k * mxu_width : (k + 1) * mxu_width]
+                    step(index + mxus * part + k, acc_out[part], [lhs] * mxus)
+
+            def finish(part):
+                away = base[:, across(part)] + popped(acc_out[part])
+                base[:, across(part)] = away
+                outbox[slot, :, :, across(part)] = away.reshape(pair, length, -1).astype(
+                    jnp.bfloat16
+                )
+
+                @pl.when(section < last)
+                def _():
                     onward(slot, part).start()
+
+            project(0)
+            for part in range(1, parts):
+                project(part)
+                finish(part - 1)
+            finish(parts - 1)
 
             @pl.when(section == last)
             def _():
+                away = base[...]
+                offset = jnp.sum(fold_lanes(away), axis=-1, keepdims=True) / width
+                square = jnp.sum(fold_lanes(away * away), axis=-1, keepdims=True) / width
+                variance = jnp.maximum(square - offset * offset, 0.0)
+                normed = (away - offset) * lax.rsqrt(variance + norm_eps) * norm[0] + norm[1]
+                outbox[slot] = normed.reshape(pair, length, -1).astype(jnp.bfloat16)
                 for core_index in range(pair):
                     if core_index == lead:
                         @pl.when(slot < last)
@@ -328,9 +424,11 @@
             return carry
 
         lax.fori_loop(0, sections, one_slot, 0)
+        drain()
 
         @pl.when(section < last)
         def _():
+            norm_onward.wait_send()
             for slot in range(sections):
                 onward_all(slot).wait_send()
 
@@ -341,7 +439,21 @@
             if lead:
                 homes_sent(last, slice(0, lead)).wait_send()
 
-    pl.when(leads)(run_section)
+    def with_accumulators(*accs):
+        pairs = [accs[start : start + mxus] for start in range(0, len(accs), mxus)]
+
+        @pl.when(leads)
+        def _():
+            run_section(pairs[0], pairs[1], pairs[2], pairs[3:])
+
+    pl.run_scoped(
+        with_accumulators,
+        *[
+            pltpu.ACC(mxu)((rows, mxu_width), jnp.float32)
+            for _ in range(3 + parts)
+            for mxu in range(mxus)
+        ],
+    )
 
     @pl.when(jnp.logical_not(first_stop))
     def _():
@@ -364,8 +476,8 @@
     lru_width = weights[0].shape[2]
     tap_count = weights[1].shape[1]
     _, blocks, block_width, _ = weights[3].shape
-    group = max(1, min(blocks, mxu_width // block_width))
-    wide = group * block_width
+    parts = width // (mxus * mxu_width)
+    assert lru_width == mxus * mxu_width and mxu_width % block_width == 0
     vmem = pltpu.VMEM
     f32, bf16 = jnp.float32, jnp.bfloat16
     return pl.pallas_call(
@@ -377,24 +489,22 @@
             vmem((width, lru_width), bf16),
             vmem((lru_width, width), bf16),
             vmem((tap_count, lru_width), f32),
-            vmem((1, lru_width), f32),
-            vmem((blocks, block_width, block_width), bf16),
-            vmem((1, lru_width), f32),
-            vmem((blocks, block_width, block_width), bf16),
-            vmem((1, lru_width), f32),
-            vmem((1, lru_width), f32),
-            vmem((1, width), f32),
-            vmem((1, width), f32),
-            vmem((blocks // group, wide, wide), bf16),
-            vmem((blocks // group, wide, wide), bf16),
+            vmem((4, 1, lru_width), f32),
+            vmem((2, blocks, block_width, block_width), bf16),
+            vmem((2, 1, width), f32),
+            vmem((2, 1, width), f32),
+            vmem((2, mxus, mxu_width, mxu_width), bf16),
+            vmem((2, 1, lru_width), f32),
+            vmem((pair * length, width), f32),
             vmem((length, width), bf16),
             vmem((sections, pair, length, width), bf16),
             vmem((sections, pair, length, width), bf16),
-            pltpu.SemaphoreType.DMA((11 + stream_parts,)),
+            pltpu.SemaphoreType.DMA((12,)),
             pltpu.SemaphoreType.DMA,
             pltpu.SemaphoreType.DMA((sections,)),
-            pltpu.SemaphoreType.DMA((sections, stream_parts)),
+            pltpu.SemaphoreType.DMA((sections, parts)),
             pltpu.SemaphoreType.DMA,
+            pltpu.SemaphoreType.DMA((2,)),
             pltpu.SemaphoreType.REGULAR,
         ],
         compiler_params=pltpu.CompilerParams(collective_id=0, has_side_effects=True),

time: 18.8 us -> 17.3 us (0.920)
  Pallas kernels: 18 us -> 16.5 us
    pallas_call x1, Pallas kernels: 18 us -> 16.5 us  [shards(): pl.pallas_call(functools.partial(stack_kernel, sections), out_shape=pltpu...]
where the time goes in v2:
time: 17.3 us; the launch traced here: 17.1 us
  Pallas kernels  16.5 us (95%)
  local copies, waits for them, and re-layouts  0.62 us (4%)
    pallas_call x1, Pallas kernels, shards(): pl.pallas_call(functools.partial(stack_kernel, sections), out_shape=pltpu...  16.5 us
    unnamed x1, local copies, waits for them, and re-layouts  0.62 us

profile of v2, /device:TPU:17, one launch (start us, length us, event | category | flops | bytes accessed | tf_op | source)
XLA Modules:
  0.0 17.1 jit_solution(8225503962185542528)
XLA Ops:
  0.0 16.5 %section_stack.1 = bf16[1,1,8,2048]{3,2,1,0:T(8,128)(2,1)S(1)} custom-call(bf16[1,1,8,2048]{3,2,1,0:T(8,128)(2,1)} %tokens_hbm.1, bf16[1,2048,512]{2,1,0:T(8,128)(2,1)} %w_in_hbm.1, f32[1,4,512]{2,1,0:T(4,128)} %taps_hbm.1, f32[1,512]{1,0:T(1,128)} %cbias_hbm.1, bf16[1,8,64,64]{3,2,1,0:T(8,128)(2,1)} %grate_hbm.1, f32[1,512]{1,0:T(1,128)} %brate_hbm.1, ...), custom_call_target="tpu_custom_call" | custom-call | tf_op jit(solution)/shard_map/section_stack/pallas_call | solution.py:483
  16.5 0.6 %copy.14 = bf16[1,1,8,2048]{3,2,1,0:T(8,128)(2,1)} copy(bf16[1,1,8,2048]{3,2,1,0:T(8,128)(2,1)S(1)} %section_stack.1) | data formatting | bytes 65536

commit v3 on v2

--- a/solution.py
+++ b/solution.py
@@ -47,7 +47,6 @@
     maps,
     folded,
     base,
-    mine,
     inbox,
     outbox,
     load_sem,
@@ -89,7 +88,7 @@
     def load(src, dst, index):
         return pltpu.make_async_copy(src, dst, load_sem.at[index])
 
-    own = load(tokens_hbm.at[0, 0], mine, 0)
+    own = load(tokens_hbm.at[0, 0], inbox.at[0, lead], 0)
     small = [
         load(grate_hbm.at[0], gates.at[0], 1),
         load(ginput_hbm.at[0], gates.at[1], 2),
@@ -101,9 +100,14 @@
         load(gain_hbm, norm.at[0], 8),
         load(shift_hbm, norm.at[1], 9),
     ]
-    load_in = load(w_in_hbm.at[0], w_in, 10)
-    load_out = load(w_out_hbm.at[0], w_out, 11)
-    own.start()
+    load_in = [
+        load(w_in_hbm.at[0, across(part)], w_in.at[across(part)], 10 + part)
+        for part in range(parts)
+    ]
+    load_out = [
+        load(w_out_hbm.at[0, :, across(part)], w_out.at[:, across(part)], 10 + parts + part)
+        for part in range(parts)
+    ]
 
     @pl.when(first_stop)
     def _():
@@ -124,28 +128,9 @@
         last_stop, sections * pair - 1, jnp.where(leads & (section > 1), 2, 1)
     ).astype(jnp.int32)
 
-    @pl.when(leads)
-    def _():
-        for copy in small:
-            copy.start()
-        load_in.start()
-        load_out.start()
-
-    @pl.when(jnp.logical_not(first_stop))
-    def _():
-        pl.semaphore_wait(barrier, heard)
-
-    @pl.when(leads & (section > 0))
-    def _():
-        pl.semaphore_signal(
-            ready_sem, inc=1, device_id=at(section - 1, lead), device_id_type=MESH
-        )
-
-    own.wait()
-
     def entry(part):
         return pltpu.make_async_remote_copy(
-            src_ref=mine.at[:, across(part)],
+            src_ref=tokens_hbm.at[0, 0, :, across(part)],
             dst_ref=inbox.at[section, core, :, across(part)],
             send_sem=entry_sem,
             recv_sem=recv_sem.at[section, part],
@@ -155,8 +140,28 @@
 
     @pl.when(jnp.logical_not(first_stop))
     def _():
+        pl.semaphore_wait(barrier, heard)
         for part in range(parts):
             entry(part).start()
+
+    @pl.when(first_stop)
+    def _():
+        own.start()
+
+    @pl.when(leads & (section > 0))
+    def _():
+        pl.semaphore_signal(
+            ready_sem, inc=1, device_id=at(section - 1, lead), device_id_type=MESH
+        )
+
+    @pl.when(leads)
+    def _():
+        for copy in small[:3]:
+            copy.start()
+        for copy in load_in:
+            copy.start()
+        for copy in small[3:] + load_out:
+            copy.start()
 
     def arrival(slot, part, cores):
         return pltpu.make_async_remote_copy(
@@ -262,10 +267,11 @@
         for copy in small:
             copy.wait()
 
-        @pl.when(section < last)
-        def _():
+        def norm_send():
             pl.semaphore_wait(ready_sem, 1)
             norm_onward.start()
+
+        pl.when((section > 0) & (section < last))(norm_send)
 
         for gate in range(2):
             for block in range(blocks):
@@ -276,17 +282,19 @@
         minus_decay = -channel[3]
         softplus = jnp.maximum(minus_decay, 0.0) + jnp.log1p(jnp.exp(-jnp.abs(minus_decay)))
         channel[3] = -decay_scale * softplus
-        load_in.wait()
-
-        @pl.when(section == 0)
+
+        @pl.when(first_stop)
         def _():
-            inbox[0, lead] = mine[...]
+            own.wait()
+            load_in[0].wait()
             before[0] = jnp.ones_like(before[0])
             before[1] = jnp.zeros_like(before[1])
             folded[...] = jnp.zeros_like(folded)
 
         @pl.when(section > 0)
         def _():
+            for copy in load_in + load_out:
+                copy.wait()
             norm_onward.wait_recv()
             which = lax.broadcasted_iota(jnp.int32, (rows, mxu_width), 0)
             for k in range(tiles_in):
@@ -308,7 +316,6 @@
             folded[1] = result[2:3] + result[3:4]
             before[1] = before[1] - jnp.mean(before[1])
 
-        load_out.wait()
         for mxu in range(mxus):
             stage(0, mxu)
             stage(1, mxu)
@@ -335,16 +342,24 @@
                 raw = inbox[slot, :, :, across(part)].astype(jnp.float32).reshape(rows, -1)
                 total = total + fold_lanes(raw)
                 squares = squares + fold_lanes(raw * raw)
+                if part + 1 < parts:
+                    pl.when(entering)(load_in[part + 1].wait)
                 scaled = (raw * before[0, :, across(part)]).astype(jnp.bfloat16)
                 for start in range(0, part_width, mxu_width):
                     lhs = scaled[:, start : start + mxu_width]
                     step(index, acc_in, [lhs] * mxus)
                     index += 1
+
             mean = jnp.sum(total, axis=-1, keepdims=True) / width
             square = jnp.sum(squares, axis=-1, keepdims=True) / width
             variance = jnp.maximum(square - mean * mean, 0.0)
             scale = jnp.where(section > 0, lax.rsqrt(variance + norm_eps), 1.0)
             lower = scale * mean
+
+            @pl.when(entering & (section < last))
+            def _():
+                norm_send()
+
             projected = popped(acc_in) * scale - lower * folded[0] + folded[1]
             projected = projected.astype(jnp.bfloat16).astype(jnp.float32)
             projected = projected.reshape(pair, length, lru_width)
@@ -356,6 +371,7 @@
                 convolved = convolved + shifted * taps[tap : tap + 1][None]
             convolved = convolved.reshape(rows, lru_width).astype(jnp.bfloat16)
             lhs = [convolved[:, m * mxu_width : (m + 1) * mxu_width] for m in range(mxus)]
+            pl.when(entering)(load_out[0].wait)
             step(index, acc_rate, lhs)
             step(index + 1, acc_input, lhs)
             index += 2
@@ -380,6 +396,8 @@
             mixed = hidden.reshape(rows, lru_width).astype(jnp.bfloat16)
 
             def project(part):
+                if part + 1 < parts:
+                    pl.when(entering)(load_out[part + 1].wait)
                 for k in range(mxus):
                     lhs = mixed[:, k * mxu_width : (k + 1) * mxu_width]
                     step(index + mxus * part + k, acc_out[part], [lhs] * mxus)
@@ -458,7 +476,7 @@
     @pl.when(jnp.logical_not(first_stop))
     def _():
         pltpu.make_async_remote_copy(
-            src_ref=mine,
+            src_ref=tokens_hbm.at[0, 0],
             dst_ref=inbox.at[section, core],
             send_sem=entry_sem,
             recv_sem=recv_sem.at[section, 0],
@@ -496,10 +514,9 @@
             vmem((2, mxus, mxu_width, mxu_width), bf16),
             vmem((2, 1, lru_width), f32),
             vmem((pair * length, width), f32),
-            vmem((length, width), bf16),
             vmem((sections, pair, length, width), bf16),
             vmem((sections, pair, length, width), bf16),
-            pltpu.SemaphoreType.DMA((12,)),
+            pltpu.SemaphoreType.DMA((10 + 2 * parts,)),
             pltpu.SemaphoreType.DMA,
             pltpu.SemaphoreType.DMA((sections,)),
             pltpu.SemaphoreType.DMA((sections, parts)),

time: 17.3 us -> 16.6 us (0.960)
  Pallas kernels: 16.5 us -> 15.8 us
    pallas_call x1, Pallas kernels: 16.5 us -> 15.8 us  [shards(): pl.pallas_call(functools.partial(stack_kernel, sections), out_shape=pltpu...]
where the time goes in v3:
time: 16.6 us; the launch traced here: 16.5 us
  Pallas kernels  15.8 us (95%)
  local copies, waits for them, and re-layouts  0.62 us (4%)
    pallas_call x1, Pallas kernels, shards(): pl.pallas_call(functools.partial(stack_kernel, sections), out_shape=pltpu...  15.8 us
    unnamed x1, local copies, waits for them, and re-layouts  0.62 us

profile of v3, /device:TPU:17, one launch (start us, length us, event | category | flops | bytes accessed | tf_op | source)
XLA Modules:
  0.0 16.5 jit_solution(9973914417480776270)
XLA Ops:
  0.0 15.8 %section_stack.1 = bf16[1,1,8,2048]{3,2,1,0:T(8,128)(2,1)S(1)} custom-call(bf16[1,1,8,2048]{3,2,1,0:T(8,128)(2,1)} %tokens_hbm.1, bf16[1,2048,512]{2,1,0:T(8,128)(2,1)} %w_in_hbm.1, f32[1,4,512]{2,1,0:T(4,128)} %taps_hbm.1, f32[1,512]{1,0:T(1,128)} %cbias_hbm.1, bf16[1,8,64,64]{3,2,1,0:T(8,128)(2,1)} %grate_hbm.1, f32[1,512]{1,0:T(1,128)} %brate_hbm.1, ...), custom_call_target="tpu_custom_call" | custom-call | tf_op jit(solution)/shard_map/section_stack/pallas_call | solution.py:501
  15.8 0.6 %copy.14 = bf16[1,1,8,2048]{3,2,1,0:T(8,128)(2,1)} copy(bf16[1,1,8,2048]{3,2,1,0:T(8,128)(2,1)S(1)} %section_stack.1) | data formatting | bytes 65536

commit v4 on v3

--- a/solution.py
+++ b/solution.py
@@ -44,6 +44,8 @@
     gates,
     norm,
     before,
+    after,
+    landing,
     maps,
     folded,
     base,
@@ -55,7 +57,9 @@
     recv_sem,
     final_sem,
     norm_sem,
+    home_sem,
     ready_sem,
+    *accs,
 ):
     section = lax.axis_index("pp")
     column = lax.axis_index("tp")
@@ -193,15 +197,42 @@
             device_id_type=MESH,
         )
 
-    def home(slot, core_index):
-        return pltpu.make_async_remote_copy(
-            src_ref=outbox.at[slot, core_index],
-            dst_ref=out_ref.at[0, 0],
+    def home(slot, part, core_index):
+        return pltpu.make_async_remote_copy(
+            src_ref=outbox.at[slot, core_index, :, across(part)],
+            dst_ref=landing.at[:, across(part)],
             send_sem=send_sem.at[slot],
             recv_sem=final_sem,
             device_id=at(slot, core_index),
             device_id_type=MESH,
         )
+
+    def landed():
+        return pltpu.make_async_remote_copy(
+            src_ref=landing,
+            dst_ref=landing,
+            send_sem=entry_sem,
+            recv_sem=final_sem,
+            device_id=at(0, lead),
+            device_id_type=MESH,
+        )
+
+    def norm_home(slot, core_index):
+        return pltpu.make_async_remote_copy(
+            src_ref=norm,
+            dst_ref=after,
+            send_sem=home_sem.at[slot, core_index],
+            recv_sem=norm_sem.at[2],
+            device_id=at(slot, core_index),
+            device_id_type=MESH,
+        )
+
+    homes = [
+        (slot, core_index)
+        for slot in range(sections)
+        for core_index in reversed(range(pair))
+        if (slot, core_index) != (last, lead)
+    ]
 
     def homes_sent(slot, cores):
         return pltpu.make_async_remote_copy(
@@ -323,6 +354,12 @@
 
         def delayed(x, by, fill):
             return jnp.where(position >= by, pltpu.roll(x, by, 1), fill)
+
+        @pl.when(section == last)
+        def _():
+            after[...] = norm[...]
+            for slot, core_index in homes:
+                norm_home(slot, core_index).start()
 
         def one_slot(slot, carry):
             entering = (section == 0) & (slot == 0)
@@ -404,7 +441,6 @@
 
             def finish(part):
                 away = base[:, across(part)] + popped(acc_out[part])
-                base[:, across(part)] = away
                 outbox[slot, :, :, across(part)] = away.reshape(pair, length, -1).astype(
                     jnp.bfloat16
                 )
@@ -412,6 +448,15 @@
                 @pl.when(section < last)
                 def _():
                     onward(slot, part).start()
+
+                @pl.when((section == last) & (slot < last))
+                def _():
+                    home(slot, part, lead).start()
+
+                for core_index in range(lead):
+                    @pl.when(section == last)
+                    def _():
+                        home(slot, part, core_index).start()
 
             project(0)
             for part in range(1, parts):
@@ -419,26 +464,6 @@
                 finish(part - 1)
             finish(parts - 1)
 
-            @pl.when(section == last)
-            def _():
-                away = base[...]
-                offset = jnp.sum(fold_lanes(away), axis=-1, keepdims=True) / width
-                square = jnp.sum(fold_lanes(away * away), axis=-1, keepdims=True) / width
-                variance = jnp.maximum(square - offset * offset, 0.0)
-                normed = (away - offset) * lax.rsqrt(variance + norm_eps) * norm[0] + norm[1]
-                outbox[slot] = normed.reshape(pair, length, -1).astype(jnp.bfloat16)
-                for core_index in range(pair):
-                    if core_index == lead:
-                        @pl.when(slot < last)
-                        def _():
-                            home(slot, core_index).start()
-
-                        @pl.when(slot == last)
-                        def _():
-                            out_ref[0, 0] = outbox[slot, core_index]
-                    else:
-                        home(slot, core_index).start()
-
             return carry
 
         lax.fori_loop(0, sections, one_slot, 0)
@@ -452,26 +477,19 @@
 
         @pl.when(section == last)
         def _():
+            landing[...] = outbox[last, lead]
+            for slot, core_index in homes:
+                norm_home(slot, core_index).wait_send()
             for slot in range(last):
                 homes_sent(slot, slice(0, pair)).wait_send()
             if lead:
                 homes_sent(last, slice(0, lead)).wait_send()
 
-    def with_accumulators(*accs):
-        pairs = [accs[start : start + mxus] for start in range(0, len(accs), mxus)]
-
-        @pl.when(leads)
-        def _():
-            run_section(pairs[0], pairs[1], pairs[2], pairs[3:])
-
-    pl.run_scoped(
-        with_accumulators,
-        *[
-            pltpu.ACC(mxu)((rows, mxu_width), jnp.float32)
-            for _ in range(3 + parts)
-            for mxu in range(mxus)
-        ],
-    )
+    pairs = [accs[start : start + mxus] for start in range(0, len(accs), mxus)]
+
+    @pl.when(leads)
+    def _():
+        run_section(pairs[0], pairs[1], pairs[2], pairs[3:])
 
     @pl.when(jnp.logical_not(first_stop))
     def _():
@@ -486,7 +504,23 @@
 
     @pl.when(jnp.logical_not(last_stop))
     def _():
-        home(0, 0).wait_recv()
+        pltpu.make_async_remote_copy(
+            src_ref=norm,
+            dst_ref=after,
+            send_sem=entry_sem,
+            recv_sem=norm_sem.at[2],
+            device_id=at(0, lead),
+            device_id_type=MESH,
+        ).wait_recv()
+        landed().wait_recv()
+
+    raw = landing[...].astype(jnp.float32)
+    mean = jnp.sum(fold_lanes(raw), axis=-1, keepdims=True) / width
+    square = jnp.sum(fold_lanes(raw * raw), axis=-1, keepdims=True) / width
+    variance = jnp.maximum(square - mean * mean, 0.0)
+    scale = lax.rsqrt(variance + norm_eps)
+    normed = (raw * scale - mean * scale) * after[0] + after[1]
+    out_ref[0, 0] = normed.astype(jnp.bfloat16)
 
 
 def shards(sections, pair, tokens_in, *weights):
@@ -498,8 +532,27 @@
     assert lru_width == mxus * mxu_width and mxu_width % block_width == 0
     vmem = pltpu.VMEM
     f32, bf16 = jnp.float32, jnp.bfloat16
+    scoped = [
+        pltpu.SemaphoreType.DMA((10 + 2 * parts,)),
+        pltpu.SemaphoreType.DMA,
+        pltpu.SemaphoreType.DMA((sections,)),
+        pltpu.SemaphoreType.DMA((sections, parts)),
+        pltpu.SemaphoreType.DMA,
+        pltpu.SemaphoreType.DMA((3,)),
+        pltpu.SemaphoreType.DMA((sections, pair)),
+        pltpu.SemaphoreType.REGULAR,
+        *[
+            pltpu.ACC(mxu)((pair * length, mxu_width), jnp.float32)
+            for _ in range(3 + parts)
+            for mxu in range(mxus)
+        ],
+    ]
+
+    def kernel(*refs):
+        pl.run_scoped(functools.partial(stack_kernel, sections, *refs), *scoped)
+
     return pl.pallas_call(
-        functools.partial(stack_kernel, sections),
+        kernel,
         out_shape=pltpu.VMEM(tokens_in.shape, tokens_in.dtype),
         in_specs=[pl.BlockSpec(memory_space=pl.ANY)] * (1 + len(weights)),
         out_specs=pl.BlockSpec(memory_space=pltpu.VMEM),
@@ -511,18 +564,13 @@
             vmem((2, blocks, block_width, block_width), bf16),
             vmem((2, 1, width), f32),
             vmem((2, 1, width), f32),
+            vmem((2, 1, width), f32),
+            vmem((length, width), bf16),
             vmem((2, mxus, mxu_width, mxu_width), bf16),
             vmem((2, 1, lru_width), f32),
             vmem((pair * length, width), f32),
             vmem((sections, pair, length, width), bf16),
             vmem((sections, pair, length, width), bf16),
-            pltpu.SemaphoreType.DMA((10 + 2 * parts,)),
-            pltpu.SemaphoreType.DMA,
-            pltpu.SemaphoreType.DMA((sections,)),
-            pltpu.SemaphoreType.DMA((sections, parts)),
-            pltpu.SemaphoreType.DMA,
-            pltpu.SemaphoreType.DMA((2,)),
-            pltpu.SemaphoreType.REGULAR,
         ],
         compiler_params=pltpu.CompilerParams(collective_id=0, has_side_effects=True),
         name="section_stack",

time: 16.6 us -> 16 us (0.964)
  Pallas kernels: 15.8 us -> 15.3 us
    pallas_call x1, Pallas kernels: 15.8 us -> 15.3 us  [shards(): pl.pallas_call(kernel, out_shape=pltpu.VMEM(tokens_in.shape, tokens_in.dt...]
where the time goes in v4:
time: 16 us; the launch traced here: 15.9 us
  Pallas kernels  15.3 us (96%)
  local copies, waits for them, and re-layouts  0.62 us (4%)
    pallas_call x1, Pallas kernels, shards(): pl.pallas_call(kernel, out_shape=pltpu.VMEM(tokens_in.shape, tokens_in.dt...  15.3 us
    unnamed x1, local copies, waits for them, and re-layouts  0.62 us

profile of v4, /device:TPU:17, one launch (start us, length us, event | category | flops | bytes accessed | tf_op | source)
XLA Modules:
  0.0 15.9 jit_solution(18192417290815458268)
XLA Ops:
  0.0 15.3 %section_stack.1 = bf16[1,1,8,2048]{3,2,1,0:T(8,128)(2,1)S(1)} custom-call(bf16[1,1,8,2048]{3,2,1,0:T(8,128)(2,1)} %refs_0_.1, bf16[1,2048,512]{2,1,0:T(8,128)(2,1)} %refs_1_.1, f32[1,4,512]{2,1,0:T(4,128)} %refs_2_.1, f32[1,512]{1,0:T(1,128)} %refs_3_.1, bf16[1,8,64,64]{3,2,1,0:T(8,128)(2,1)} %refs_4_.1, f32[1,512]{1,0:T(1,128)} %refs_5_.1, ...), custom_call_target="tpu_custom_call" | custom-call | tf_op jit(solution)/shard_map/section_stack/pallas_call | solution.py:554
  15.3 0.6 %copy.14 = bf16[1,1,8,2048]{3,2,1,0:T(8,128)(2,1)} copy(bf16[1,1,8,2048]{3,2,1,0:T(8,128)(2,1)S(1)} %section_stack.1) | data formatting | bytes 65536

commit v5 on v4

--- a/solution.py
+++ b/solution.py
@@ -12,6 +12,7 @@
 mxu_width = 256
 mxus = 2
 lanes = 128
+smallest = 1e-30
 MESH = pl.DeviceIdType.MESH
 
 
@@ -48,6 +49,7 @@
     landing,
     maps,
     folded,
+    masked,
     base,
     inbox,
     outbox,
@@ -272,9 +274,12 @@
     def stage(index, mxu):
         pltpu.matmul_push_rhs(unit(index, mxu), staging_register=index % 2, mxu_index=mxu)
 
-    def step(index, accs, lhs):
+    def multiply(index, accs, lhs):
         for mxu in range(mxus):
             pltpu.matmul_acc_lhs(accs[mxu], lhs[mxu], load_staged_rhs=index % 2)
+
+    def step(index, accs, lhs):
+        multiply(index, accs, lhs)
         for mxu in range(mxus):
             stage(index + 2, mxu)
 
@@ -307,12 +312,18 @@
         for gate in range(2):
             for block in range(blocks):
                 to = (block % group) * block_width
-                maps[gate, block // group, to : to + block_width, to : to + block_width] = gates[
-                    gate, block
-                ]
+                maps[gate, block // group, to : to + block_width, to : to + block_width] = (
+                    gates[gate, block] * 0.5
+                )
         minus_decay = -channel[3]
         softplus = jnp.maximum(minus_decay, 0.0) + jnp.log1p(jnp.exp(-jnp.abs(minus_decay)))
-        channel[3] = -decay_scale * softplus
+        channel[3] = -0.5 * decay_scale * softplus
+        channel[1] = 0.5 * channel[1]
+        channel[2] = 0.5 * channel[2]
+        position = lax.broadcasted_iota(jnp.int32, (length, lru_width), 0)
+        tap_count = taps.shape[0]
+        for tap in range(tap_count):
+            masked[tap] = jnp.where(position >= tap_count - 1 - tap, taps[tap : tap + 1], 0.0)
 
         @pl.when(first_stop)
         def _():
@@ -350,11 +361,6 @@
         for mxu in range(mxus):
             stage(0, mxu)
             stage(1, mxu)
-        position = lax.broadcasted_iota(jnp.int32, (pair, length, lru_width), 1)
-
-        def delayed(x, by, fill):
-            return jnp.where(position >= by, pltpu.roll(x, by, 1), fill)
-
         @pl.when(section == last)
         def _():
             after[...] = norm[...]
@@ -393,22 +399,21 @@
             scale = jnp.where(section > 0, lax.rsqrt(variance + norm_eps), 1.0)
             lower = scale * mean
 
-            @pl.when(entering & (section < last))
+            @pl.when(entering)
             def _():
-                norm_send()
+                pl.when(section < last)(norm_send)
+                for copy in load_out[:2]:
+                    copy.wait()
 
             projected = popped(acc_in) * scale - lower * folded[0] + folded[1]
             projected = projected.astype(jnp.bfloat16).astype(jnp.float32)
             projected = projected.reshape(pair, length, lru_width)
-            tap_count = taps.shape[0]
-            convolved = channel[0][None]
-            for tap in range(tap_count):
-                by = tap_count - 1 - tap
-                shifted = delayed(projected, by, 0.0) if by else projected
-                convolved = convolved + shifted * taps[tap : tap + 1][None]
+            convolved = channel[0][None] + projected * masked[tap_count - 1][None]
+            for by in range(1, tap_count):
+                delayed = pltpu.roll(projected, by, 1)
+                convolved = convolved + delayed * masked[tap_count - 1 - by][None]
             convolved = convolved.reshape(rows, lru_width).astype(jnp.bfloat16)
             lhs = [convolved[:, m * mxu_width : (m + 1) * mxu_width] for m in range(mxus)]
-            pl.when(entering)(load_out[0].wait)
             step(index, acc_rate, lhs)
             step(index + 1, acc_input, lhs)
             index += 2
@@ -416,28 +421,34 @@
                 raw = inbox[slot, :, :, across(part)].astype(jnp.float32).reshape(rows, -1)
                 gain, shift = before[0, :, across(part)], before[1, :, across(part)]
                 base[:, across(part)] = (raw * scale - lower) * gain + shift
-            rate_gate = jax.nn.sigmoid(popped(acc_rate) + channel[1])
-            input_gate = jax.nn.sigmoid(popped(acc_input) + channel[2])
-            log_decay = rate_gate * channel[3]
+            rate = jnp.tanh(popped(acc_rate) + channel[1])
+            log_decay = rate * channel[3] + channel[3]
             decay = jnp.exp(log_decay)
-            scale_in = jnp.sqrt(-jnp.tanh(log_decay) * (decay * decay + 1.0))
-            hidden = scale_in * input_gate * convolved.astype(jnp.float32)
-            hidden = hidden.reshape(pair, length, lru_width)
-            decay = decay.reshape(pair, length, lru_width)
+            gap = -jnp.tanh(log_decay) * (decay * decay + 1.0)
+            scale_in = gap * lax.rsqrt(jnp.maximum(gap, smallest))
+            half = 0.5 * convolved.astype(jnp.float32)
+            gated = jnp.tanh(popped(acc_input) + channel[2]) * half + half
+            hidden = (scale_in * gated).reshape(pair, length, lru_width)
+            decay = jnp.where(
+                position[None] >= 1, decay.reshape(pair, length, lru_width), 0.0
+            )
             by = 1
             while by < length:
-                hidden = decay * delayed(hidden, by, 0.0) + hidden
+                hidden = decay * pltpu.roll(hidden, by, 1) + hidden
                 if 2 * by < length:
-                    decay = decay * delayed(decay, by, 1.0)
+                    decay = decay * pltpu.roll(decay, by, 1)
                 by *= 2
             mixed = hidden.reshape(rows, lru_width).astype(jnp.bfloat16)
 
             def project(part):
-                if part + 1 < parts:
-                    pl.when(entering)(load_out[part + 1].wait)
                 for k in range(mxus):
                     lhs = mixed[:, k * mxu_width : (k + 1) * mxu_width]
-                    step(index + mxus * part + k, acc_out[part], [lhs] * mxus)
+                    multiply(index + mxus * part + k, acc_out[part], [lhs] * mxus)
+
+            def prepare(part):
+                for k in range(2):
+                    for mxu in range(mxus):
+                        stage(index + mxus * part + k, mxu)
 
             def finish(part):
                 away = base[:, across(part)] + popped(acc_out[part])
@@ -460,8 +471,13 @@
 
             project(0)
             for part in range(1, parts):
+                prepare(part)
                 project(part)
                 finish(part - 1)
+                if part == 1:
+                    for copy in load_out[2:]:
+                        pl.when(entering)(copy.wait)
+            prepare(parts)
             finish(parts - 1)
 
             return carry
@@ -568,6 +584,7 @@
             vmem((length, width), bf16),
             vmem((2, mxus, mxu_width, mxu_width), bf16),
             vmem((2, 1, lru_width), f32),
+            vmem((tap_count, length, lru_width), f32),
             vmem((pair * length, width), f32),
             vmem((sections, pair, length, width), bf16),
             vmem((sections, pair, length, width), bf16),

time: 16 us -> 15.8 us (0.988)
  Pallas kernels: 15.3 us -> 15 us
    pallas_call x1, Pallas kernels: 15.3 us -> 15 us  [shards(): pl.pallas_call(kernel, out_shape=pltpu.VMEM(tokens_in.shape, tokens_in.dt...]
where the time goes in v5:
time: 15.8 us; the launch traced here: 15.7 us
  Pallas kernels  15 us (95%)
  local copies, waits for them, and re-layouts  0.62 us (4%)
    pallas_call x1, Pallas kernels, shards(): pl.pallas_call(kernel, out_shape=pltpu.VMEM(tokens_in.shape, tokens_in.dt...  15 us
    unnamed x1, local copies, waits for them, and re-layouts  0.62 us

profile of v5, /device:TPU:17, one launch (start us, length us, event | category | flops | bytes accessed | tf_op | source)
XLA Modules:
  0.0 15.7 jit_solution(9299659377398557174)
XLA Ops:
  0.0 15.0 %section_stack.1 = bf16[1,1,8,2048]{3,2,1,0:T(8,128)(2,1)S(1)} custom-call(bf16[1,1,8,2048]{3,2,1,0:T(8,128)(2,1)} %refs_0_.1, bf16[1,2048,512]{2,1,0:T(8,128)(2,1)} %refs_1_.1, f32[1,4,512]{2,1,0:T(4,128)} %refs_2_.1, f32[1,512]{1,0:T(1,128)} %refs_3_.1, bf16[1,8,64,64]{3,2,1,0:T(8,128)(2,1)} %refs_4_.1, f32[1,512]{1,0:T(1,128)} %refs_5_.1, ...), custom_call_target="tpu_custom_call" | custom-call | tf_op jit(solution)/shard_map/section_stack/pallas_call | solution.py:570
  15.0 0.6 %copy.14 = bf16[1,1,8,2048]{3,2,1,0:T(8,128)(2,1)} copy(bf16[1,1,8,2048]{3,2,1,0:T(8,128)(2,1)S(1)} %section_stack.1) | data formatting | bytes 65536

commit v6 on v5

--- a/solution.py
+++ b/solution.py
@@ -13,6 +13,7 @@
 mxus = 2
 lanes = 128
 smallest = 1e-30
+log2_e = 1.4426950408889634
 MESH = pl.DeviceIdType.MESH
 
 
@@ -69,7 +70,7 @@
     pair, length = inbox.shape[1:3]
     rows = pair * length
     width, lru_width = w_in.shape
-    parts = recv_sem.shape[1]
+    parts = recv_sem.shape[2]
     part_width = width // parts
     tiles_in = width // mxu_width
     core = lax.rem(column, pair)
@@ -139,7 +140,7 @@
             src_ref=tokens_hbm.at[0, 0, :, across(part)],
             dst_ref=inbox.at[section, core, :, across(part)],
             send_sem=entry_sem,
-            recv_sem=recv_sem.at[section, part],
+            recv_sem=recv_sem.at[section, 0, part],
             device_id=at(0, lead),
             device_id_type=MESH,
         )
@@ -162,29 +163,16 @@
 
     @pl.when(leads)
     def _():
-        for copy in small[:3]:
+        for copy in small + load_in + load_out:
             copy.start()
-        for copy in load_in:
-            copy.start()
-        for copy in small[3:] + load_out:
-            copy.start()
-
-    def arrival(slot, part, cores):
+
+    def onward(slot, first, count, part):
+        cores = pl.ds(first, count)
         return pltpu.make_async_remote_copy(
             src_ref=outbox.at[slot, cores, :, across(part)],
             dst_ref=inbox.at[slot, cores, :, across(part)],
-            send_sem=entry_sem,
-            recv_sem=recv_sem.at[slot, part],
-            device_id=at(0, lead),
-            device_id_type=MESH,
-        )
-
-    def onward(slot, part):
-        return pltpu.make_async_remote_copy(
-            src_ref=outbox.at[slot, :, :, across(part)],
-            dst_ref=inbox.at[slot, :, :, across(part)],
             send_sem=send_sem.at[slot],
-            recv_sem=recv_sem.at[slot, part],
+            recv_sem=recv_sem.at[slot, first, part],
             device_id=at(jnp.minimum(section + 1, last), lead),
             device_id_type=MESH,
         )
@@ -194,12 +182,12 @@
             src_ref=outbox.at[slot],
             dst_ref=inbox.at[slot],
             send_sem=send_sem.at[slot],
-            recv_sem=recv_sem.at[slot, 0],
+            recv_sem=recv_sem.at[slot, 0, 0],
             device_id=at(jnp.minimum(section + 1, last), lead),
             device_id_type=MESH,
         )
 
-    def home(slot, part, core_index):
+    def home(slot, core_index, part):
         return pltpu.make_async_remote_copy(
             src_ref=outbox.at[slot, core_index, :, across(part)],
             dst_ref=landing.at[:, across(part)],
@@ -286,17 +274,17 @@
     def popped(accs):
         return jnp.concatenate([pltpu.matmul_pop(acc) for acc in accs], axis=1)
 
-    def run_section(acc_in, acc_rate, acc_input, acc_out):
+    def run_section(accs):
         def drain():
-            nothing = jnp.zeros((rows, mxu_width), jnp.bfloat16)
+            nothing = jnp.zeros((rows, mxu_width), jnp.float32)
             for mxu in range(mxus):
                 for register in range(2):
-                    pltpu.matmul_acc_lhs(acc_in[mxu], nothing, load_staged_rhs=register)
-            popped(acc_in)
+                    pltpu.matmul_acc_lhs(accs[0][mxu], nothing, load_staged_rhs=register)
+            popped(accs[0])
 
         drain()
-        for accs in (acc_rate, acc_input, *acc_out):
-            popped(accs)
+        for acc in accs[1:]:
+            popped(acc)
         _, blocks, block_width, _ = gates.shape
         group = mxu_width // block_width
         maps[...] = jnp.zeros_like(maps)
@@ -317,7 +305,7 @@
                 )
         minus_decay = -channel[3]
         softplus = jnp.maximum(minus_decay, 0.0) + jnp.log1p(jnp.exp(-jnp.abs(minus_decay)))
-        channel[3] = -0.5 * decay_scale * softplus
+        channel[3] = 0.5 * decay_scale * softplus
         channel[1] = 0.5 * channel[1]
         channel[2] = 0.5 * channel[2]
         position = lax.broadcasted_iota(jnp.int32, (length, lru_width), 0)
@@ -349,11 +337,10 @@
                 lhs = jnp.zeros((rows, mxu_width), jnp.float32)
                 for row, value in enumerate(split):
                     lhs = jnp.where(which == row, value, lhs)
-                lhs = lhs.astype(jnp.bfloat16)
                 for mxu in range(mxus):
                     stage(k, mxu)
-                    pltpu.matmul_acc_lhs(acc_in[mxu], lhs, load_staged_rhs=k % 2)
-            result = popped(acc_in)
+                    pltpu.matmul_acc_lhs(accs[0][mxu], lhs, load_staged_rhs=k % 2)
+            result = popped(accs[0])
             folded[0] = result[0:1] + result[1:2]
             folded[1] = result[2:3] + result[3:4]
             before[1] = before[1] - jnp.mean(before[1])
@@ -367,78 +354,87 @@
             for slot, core_index in homes:
                 norm_home(slot, core_index).start()
 
-        def one_slot(slot, carry):
-            entering = (section == 0) & (slot == 0)
-            total = jnp.zeros((rows, lanes), jnp.float32)
-            squares = jnp.zeros((rows, lanes), jnp.float32)
+        def unit_of(slot, first, count, accs, opening):
+            acc_in, acc_rate, acc_input, *acc_out = accs
+            flat, deep = (count * length, -1), (count, length, -1)
+            cores = pl.ds(first, count)
+
+            def received(part):
+                raw = inbox[slot, cores, :, across(part)]
+                return raw.astype(jnp.float32).reshape(flat)
+
+            def early(*copies):
+                if opening:
+                    @pl.when(section == 0)
+                    def _():
+                        for copy in copies:
+                            copy.wait()
+
+            total = jnp.zeros((count * length, lanes), jnp.float32)
+            squares = jnp.zeros((count * length, lanes), jnp.float32)
             index = 0
             for part in range(parts):
-                @pl.when(jnp.logical_not(entering))
-                def _():
-                    arrival(slot, part, slice(0, pair)).wait_recv()
-
-                if lead:
-                    @pl.when(entering)
+                if opening:
+                    @pl.when(section > 0)
                     def _():
-                        arrival(slot, part, slice(0, lead)).wait_recv()
-
-                raw = inbox[slot, :, :, across(part)].astype(jnp.float32).reshape(rows, -1)
+                        onward(slot, first, count, part).wait_recv()
+
+                    for other in range(lead):
+                        @pl.when(section == 0)
+                        def _():
+                            onward(slot, other, 1, part).wait_recv()
+
+                    early(*load_in[part + 1 : part + 2])
+                else:
+                    onward(slot, first, count, part).wait_recv()
+                raw = received(part)
                 total = total + fold_lanes(raw)
                 squares = squares + fold_lanes(raw * raw)
-                if part + 1 < parts:
-                    pl.when(entering)(load_in[part + 1].wait)
                 scaled = (raw * before[0, :, across(part)]).astype(jnp.bfloat16)
                 for start in range(0, part_width, mxu_width):
                     lhs = scaled[:, start : start + mxu_width]
                     step(index, acc_in, [lhs] * mxus)
                     index += 1
-
             mean = jnp.sum(total, axis=-1, keepdims=True) / width
             square = jnp.sum(squares, axis=-1, keepdims=True) / width
             variance = jnp.maximum(square - mean * mean, 0.0)
             scale = jnp.where(section > 0, lax.rsqrt(variance + norm_eps), 1.0)
             lower = scale * mean
-
-            @pl.when(entering)
-            def _():
-                pl.when(section < last)(norm_send)
-                for copy in load_out[:2]:
-                    copy.wait()
-
-            projected = popped(acc_in) * scale - lower * folded[0] + folded[1]
-            projected = projected.astype(jnp.bfloat16).astype(jnp.float32)
-            projected = projected.reshape(pair, length, lru_width)
-            convolved = channel[0][None] + projected * masked[tap_count - 1][None]
+            constant = folded[1] - lower * folded[0]
+            projected = popped(acc_in) * scale + constant
+            projected = projected.reshape(deep)
+            convolved = channel[0] + projected * masked[tap_count - 1]
             for by in range(1, tap_count):
                 delayed = pltpu.roll(projected, by, 1)
-                convolved = convolved + delayed * masked[tap_count - 1 - by][None]
-            convolved = convolved.reshape(rows, lru_width).astype(jnp.bfloat16)
-            lhs = [convolved[:, m * mxu_width : (m + 1) * mxu_width] for m in range(mxus)]
+                convolved = convolved + delayed * masked[tap_count - 1 - by]
+            convolved = convolved.reshape(flat)
+            rounded = convolved.astype(jnp.bfloat16)
+            lhs = [rounded[:, m * mxu_width : (m + 1) * mxu_width] for m in range(mxus)]
+            early(load_out[0])
             step(index, acc_rate, lhs)
             step(index + 1, acc_input, lhs)
             index += 2
             for part in range(parts):
-                raw = inbox[slot, :, :, across(part)].astype(jnp.float32).reshape(rows, -1)
                 gain, shift = before[0, :, across(part)], before[1, :, across(part)]
-                base[:, across(part)] = (raw * scale - lower) * gain + shift
+                base[: count * length, across(part)] = (
+                    received(part) * scale - lower
+                ) * gain + shift
             rate = jnp.tanh(popped(acc_rate) + channel[1])
-            log_decay = rate * channel[3] + channel[3]
-            decay = jnp.exp(log_decay)
-            gap = -jnp.tanh(log_decay) * (decay * decay + 1.0)
+            fall = rate * channel[3] + channel[3]
+            decay = jnp.exp2(fall * -log2_e)
+            gap = jnp.tanh(fall) * (decay * decay + 1.0)
             scale_in = gap * lax.rsqrt(jnp.maximum(gap, smallest))
-            half = 0.5 * convolved.astype(jnp.float32)
+            half = 0.5 * convolved
             gated = jnp.tanh(popped(acc_input) + channel[2]) * half + half
-            hidden = (scale_in * gated).reshape(pair, length, lru_width)
-            decay = jnp.where(
-                position[None] >= 1, decay.reshape(pair, length, lru_width), 0.0
-            )
+            hidden = (scale_in * gated).reshape(deep)
+            decay = jnp.where(position >= 1, decay.reshape(deep), 0.0)
             by = 1
             while by < length:
                 hidden = decay * pltpu.roll(hidden, by, 1) + hidden
                 if 2 * by < length:
                     decay = decay * pltpu.roll(decay, by, 1)
                 by *= 2
-            mixed = hidden.reshape(rows, lru_width).astype(jnp.bfloat16)
+            mixed = hidden.reshape(flat).astype(jnp.bfloat16)
 
             def project(part):
                 for k in range(mxus):
@@ -451,38 +447,48 @@
                         stage(index + mxus * part + k, mxu)
 
             def finish(part):
-                away = base[:, across(part)] + popped(acc_out[part])
-                outbox[slot, :, :, across(part)] = away.reshape(pair, length, -1).astype(
-                    jnp.bfloat16
-                )
+                away = base[: count * length, across(part)] + popped(acc_out[part])
+                outbox[slot, cores, :, across(part)] = away.reshape(deep).astype(jnp.bfloat16)
 
                 @pl.when(section < last)
                 def _():
-                    onward(slot, part).start()
+                    onward(slot, first, count, part).start()
 
                 @pl.when((section == last) & (slot < last))
                 def _():
-                    home(slot, part, lead).start()
-
-                for core_index in range(lead):
-                    @pl.when(section == last)
-                    def _():
-                        home(slot, part, core_index).start()
-
+                    home(slot, lead, part).start()
+
+                held = range(part - 1, part + 1) if part == parts - 1 else [part]
+                for core_index in range(lead if part != parts - 2 else 0):
+                    for ready_part in held:
+                        @pl.when(section == last)
+                        def _():
+                            home(slot, core_index, ready_part).start()
+
+            early(load_out[1])
             project(0)
-            for part in range(1, parts):
+            prepare(1)
+            project(1)
+            if opening:
+                pl.when((section == 0) & (section < last))(norm_send)
+            finish(0)
+            early(*load_out[2:])
+            for part in range(2, parts):
                 prepare(part)
                 project(part)
-                finish(part - 1)
-                if part == 1:
-                    for copy in load_out[2:]:
-                        pl.when(entering)(copy.wait)
+                if part < parts - 1:
+                    finish(part - 1)
             prepare(parts)
+            finish(parts - 2)
             finish(parts - 1)
 
+        unit_of(0, 0, pair, accs, True)
+
+        def one_slot(slot, carry):
+            unit_of(slot, 0, pair, accs, False)
             return carry
 
-        lax.fori_loop(0, sections, one_slot, 0)
+        lax.fori_loop(1, sections, one_slot, 0)
         drain()
 
         @pl.when(section < last)
@@ -505,7 +511,7 @@
 
     @pl.when(leads)
     def _():
-        run_section(pairs[0], pairs[1], pairs[2], pairs[3:])
+        run_section(pairs)
 
     @pl.when(jnp.logical_not(first_stop))
     def _():
@@ -513,7 +519,7 @@
             src_ref=tokens_hbm.at[0, 0],
             dst_ref=inbox.at[section, core],
             send_sem=entry_sem,
-            recv_sem=recv_sem.at[section, 0],
+            recv_sem=recv_sem.at[section, 0, 0],
             device_id=at(0, lead),
             device_id_type=MESH,
         ).wait_send()
@@ -552,7 +558,7 @@
         pltpu.SemaphoreType.DMA((10 + 2 * parts,)),
         pltpu.SemaphoreType.DMA,
         pltpu.SemaphoreType.DMA((sections,)),
-        pltpu.SemaphoreType.DMA((sections, parts)),
+        pltpu.SemaphoreType.DMA((sections, pair, parts)),
         pltpu.SemaphoreType.DMA,
         pltpu.SemaphoreType.DMA((3,)),
         pltpu.SemaphoreType.DMA((sections, pair)),

time: 15.8 us -> 15.6 us (0.987)
  Pallas kernels: 15 us -> 14.8 us
    pallas_call x1, Pallas kernels: 15 us -> 14.8 us  [shards(): pl.pallas_call(kernel, out_shape=pltpu.VMEM(tokens_in.shape, tokens_in.dt...]
where the time goes in v6:
time: 15.6 us; the launch traced here: 15.5 us
  Pallas kernels  14.8 us (95%)
  local copies, waits for them, and re-layouts  0.62 us (4%)
    pallas_call x1, Pallas kernels, shards(): pl.pallas_call(kernel, out_shape=pltpu.VMEM(tokens_in.shape, tokens_in.dt...  14.8 us
    unnamed x1, local copies, waits for them, and re-layouts  0.62 us

profile of v6, /device:TPU:17, one launch (start us, length us, event | category | flops | bytes accessed | tf_op | source)
XLA Modules:
  0.0 15.5 jit_solution(3592259207689135779)
XLA Ops:
  0.0 14.8 %section_stack.1 = bf16[1,1,8,2048]{3,2,1,0:T(8,128)(2,1)S(1)} custom-call(bf16[1,1,8,2048]{3,2,1,0:T(8,128)(2,1)} %refs_0_.1, bf16[1,2048,512]{2,1,0:T(8,128)(2,1)} %refs_1_.1, f32[1,4,512]{2,1,0:T(4,128)} %refs_2_.1, f32[1,512]{1,0:T(1,128)} %refs_3_.1, bf16[1,8,64,64]{3,2,1,0:T(8,128)(2,1)} %refs_4_.1, f32[1,512]{1,0:T(1,128)} %refs_5_.1, ...), custom_call_target="tpu_custom_call" | custom-call | tf_op jit(solution)/shard_map/section_stack/pallas_call | solution.py:576
  14.8 0.6 %copy.14 = bf16[1,1,8,2048]{3,2,1,0:T(8,128)(2,1)} copy(bf16[1,1,8,2048]{3,2,1,0:T(8,128)(2,1)S(1)} %section_stack.1) | data formatting | bytes 65536

commit v7 on v6

--- a/solution.py
+++ b/solution.py
@@ -50,6 +50,7 @@
     landing,
     maps,
     folded,
+    row_mean,
     masked,
     base,
     inbox,
@@ -111,9 +112,11 @@
         load(w_in_hbm.at[0, across(part)], w_in.at[across(part)], 10 + part)
         for part in range(parts)
     ]
+    out_cols = [slice(0, mxu_width), slice(mxu_width, part_width)]
+    out_cols += [across(part) for part in range(1, parts)]
     load_out = [
-        load(w_out_hbm.at[0, :, across(part)], w_out.at[:, across(part)], 10 + parts + part)
-        for part in range(parts)
+        load(w_out_hbm.at[0, :, cols], w_out.at[:, cols], 10 + parts + index)
+        for index, cols in enumerate(out_cols)
     ]
 
     @pl.when(first_stop)
@@ -163,7 +166,7 @@
 
     @pl.when(leads)
     def _():
-        for copy in small + load_in + load_out:
+        for copy in small + load_in[:2] + load_out[:1] + load_in[2:] + load_out[1:]:
             copy.start()
 
     def onward(slot, first, count, part):
@@ -313,37 +316,50 @@
         for tap in range(tap_count):
             masked[tap] = jnp.where(position >= tap_count - 1 - tap, taps[tap : tap + 1], 0.0)
 
+        def norm_rows(index):
+            cols = slice(index * mxu_width, (index + 1) * mxu_width)
+            which = lax.broadcasted_iota(jnp.int32, (rows, mxu_width), 0)
+            lhs = jnp.zeros((rows, mxu_width), jnp.float32)
+            for vector in range(2):
+                value = before[vector, :, cols]
+                high = value.astype(jnp.bfloat16).astype(jnp.float32)
+                lhs = jnp.where(which == 2 * vector, high, lhs)
+                lhs = jnp.where(which == 2 * vector + 1, value - high, lhs)
+            return lhs.astype(jnp.bfloat16)
+
+        def average(register):
+            load_out[0].wait()
+            ones = jnp.ones((rows, mxu_width), jnp.float32)
+            for mxu in range(mxus):
+                pltpu.matmul_push_rhs(
+                    tile(w_out, mxu, 0),
+                    staging_register=register,
+                    mxu_index=mxu,
+                    transpose=True,
+                )
+            multiply(register, accs[1], [ones] * mxus)
+
         @pl.when(first_stop)
         def _():
             own.wait()
             load_in[0].wait()
+            folded[...] = jnp.zeros_like(folded)
             before[0] = jnp.ones_like(before[0])
             before[1] = jnp.zeros_like(before[1])
-            folded[...] = jnp.zeros_like(folded)
 
         @pl.when(section > 0)
         def _():
-            for copy in load_in + load_out:
+            average(0)
+            for copy in load_in + load_out[1:]:
                 copy.wait()
             norm_onward.wait_recv()
-            which = lax.broadcasted_iota(jnp.int32, (rows, mxu_width), 0)
             for k in range(tiles_in):
-                cols = slice(k * mxu_width, (k + 1) * mxu_width)
-                split = []
-                for vector in range(2):
-                    value = before[vector, :, cols]
-                    high = value.astype(jnp.bfloat16).astype(jnp.float32)
-                    split += [high, value - high]
-                lhs = jnp.zeros((rows, mxu_width), jnp.float32)
-                for row, value in enumerate(split):
-                    lhs = jnp.where(which == row, value, lhs)
                 for mxu in range(mxus):
                     stage(k, mxu)
-                    pltpu.matmul_acc_lhs(accs[0][mxu], lhs, load_staged_rhs=k % 2)
+                multiply(k, accs[0], [norm_rows(k)] * mxus)
             result = popped(accs[0])
             folded[0] = result[0:1] + result[1:2]
             folded[1] = result[2:3] + result[3:4]
-            before[1] = before[1] - jnp.mean(before[1])
 
         for mxu in range(mxus):
             stage(0, mxu)
@@ -393,8 +409,14 @@
                 scaled = (raw * before[0, :, across(part)]).astype(jnp.bfloat16)
                 for start in range(0, part_width, mxu_width):
                     lhs = scaled[:, start : start + mxu_width]
-                    step(index, acc_in, [lhs] * mxus)
+                    multiply(index, acc_in, [lhs] * mxus)
+                    if opening and index == tiles_in // 2 - 1:
+                        pl.when(section == 0)(functools.partial(average, index % 2))
+                    for mxu in range(mxus):
+                        stage(index + 2, mxu)
                     index += 1
+            if opening:
+                row_mean[...] = popped(accs[1])[0:1] * (1.0 / mxu_width)
             mean = jnp.sum(total, axis=-1, keepdims=True) / width
             square = jnp.sum(squares, axis=-1, keepdims=True) / width
             variance = jnp.maximum(square - mean * mean, 0.0)
@@ -410,15 +432,16 @@
             convolved = convolved.reshape(flat)
             rounded = convolved.astype(jnp.bfloat16)
             lhs = [rounded[:, m * mxu_width : (m + 1) * mxu_width] for m in range(mxus)]
-            early(load_out[0])
+            early(load_out[1])
             step(index, acc_rate, lhs)
             step(index + 1, acc_input, lhs)
             index += 2
             for part in range(parts):
                 gain, shift = before[0, :, across(part)], before[1, :, across(part)]
-                base[: count * length, across(part)] = (
-                    received(part) * scale - lower
-                ) * gain + shift
+                stream = (received(part) * scale - lower) * gain + shift
+                base[: count * length, across(part)] = stream
+                if part == 0:
+                    common = fold_lanes(stream[:, :mxu_width]) * (1.0 / mxu_width)
             rate = jnp.tanh(popped(acc_rate) + channel[1])
             fall = rate * channel[3] + channel[3]
             decay = jnp.exp2(fall * -log2_e)
@@ -434,7 +457,10 @@
                 if 2 * by < length:
                     decay = decay * pltpu.roll(decay, by, 1)
                 by *= 2
-            mixed = hidden.reshape(flat).astype(jnp.bfloat16)
+            mixed = hidden.reshape(flat)
+            common = common + fold_lanes(mixed * row_mean[...])
+            common = jnp.sum(common, axis=-1, keepdims=True)
+            mixed = mixed.astype(jnp.bfloat16)
 
             def project(part):
                 for k in range(mxus):
@@ -447,32 +473,32 @@
                         stage(index + mxus * part + k, mxu)
 
             def finish(part):
-                away = base[: count * length, across(part)] + popped(acc_out[part])
+                away = base[: count * length, across(part)] - common + popped(acc_out[part])
                 outbox[slot, cores, :, across(part)] = away.reshape(deep).astype(jnp.bfloat16)
 
                 @pl.when(section < last)
                 def _():
                     onward(slot, first, count, part).start()
 
-                @pl.when((section == last) & (slot < last))
-                def _():
-                    home(slot, lead, part).start()
-
+                ahead = [lead] if not opening else list(range(lead))
+                behind = list(range(lead)) if not opening else [lead]
                 held = range(part - 1, part + 1) if part == parts - 1 else [part]
-                for core_index in range(lead if part != parts - 2 else 0):
-                    for ready_part in held:
-                        @pl.when(section == last)
-                        def _():
-                            home(slot, core_index, ready_part).start()
-
-            early(load_out[1])
+                sends = [(core_index, part) for core_index in ahead]
+                if part != parts - 2:
+                    sends += [(core_index, late) for core_index in behind for late in held]
+                for core_index, ready_part in sends:
+                    @pl.when((section == last) & ((slot < last) | (core_index < lead)))
+                    def _():
+                        home(slot, core_index, ready_part).start()
+
+            early(load_out[2])
             project(0)
             prepare(1)
             project(1)
             if opening:
                 pl.when((section == 0) & (section < last))(norm_send)
             finish(0)
-            early(*load_out[2:])
+            early(*load_out[3:])
             for part in range(2, parts):
                 prepare(part)
                 project(part)
@@ -555,7 +581,7 @@
     vmem = pltpu.VMEM
     f32, bf16 = jnp.float32, jnp.bfloat16
     scoped = [
-        pltpu.SemaphoreType.DMA((10 + 2 * parts,)),
+        pltpu.SemaphoreType.DMA((11 + 2 * parts,)),
         pltpu.SemaphoreType.DMA,
         pltpu.SemaphoreType.DMA((sections,)),
         pltpu.SemaphoreType.DMA((sections, pair, parts)),
@@ -590,6 +616,7 @@
             vmem((length, width), bf16),
             vmem((2, mxus, mxu_width, mxu_width), bf16),
             vmem((2, 1, lru_width), f32),
+            vmem((1, lru_width), f32),
             vmem((tap_count, length, lru_width), f32),
             vmem((pair * length, width), f32),
             vmem((sections, pair, length, width), bf16),

time: 15.6 us -> 15.8 us (1.013)
  the two profiles are of different devices: /device:TPU:17 before, /device:TPU:0 now
where the time goes in v7:
time: 15.8 us; the launch traced here: 15.7 us
  Pallas kernels  15.1 us (96%)
  local copies, waits for them, and re-layouts  0.62 us (4%)
    pallas_call x1, Pallas kernels, shards(): pl.pallas_call(kernel, out_shape=pltpu.VMEM(tokens_in.shape, tokens_in.dt...  15.1 us
    unnamed x1, local copies, waits for them, and re-layouts  0.62 us

profile of v7, /device:TPU:0, one launch (start us, length us, event | category | flops | bytes accessed | tf_op | source)
XLA Modules:
  0.0 15.7 jit_solution(6053256225229682586)
XLA Ops:
  0.0 15.1 %section_stack.1 = bf16[1,1,8,2048]{3,2,1,0:T(8,128)(2,1)S(1)} custom-call(bf16[1,1,8,2048]{3,2,1,0:T(8,128)(2,1)} %refs_0_.1, bf16[1,2048,512]{2,1,0:T(8,128)(2,1)} %refs_1_.1, f32[1,4,512]{2,1,0:T(4,128)} %refs_2_.1, f32[1,512]{1,0:T(1,128)} %refs_3_.1, bf16[1,8,64,64]{3,2,1,0:T(8,128)(2,1)} %refs_4_.1, f32[1,512]{1,0:T(1,128)} %refs_5_.1, ...), custom_call_target="tpu_custom_call" | custom-call | tf_op jit(solution)/shard_map/section_stack/pallas_call | solution.py:602
  15.1 0.6 %copy.14 = bf16[1,1,8,2048]{3,2,1,0:T(8,128)(2,1)} copy(bf16[1,1,8,2048]{3,2,1,0:T(8,128)(2,1)S(1)} %section_stack.1) | data formatting | bytes 65536

commit v8 on v7

--- a/solution.py
+++ b/solution.py
@@ -491,8 +491,8 @@
                     def _():
                         home(slot, core_index, ready_part).start()
 
+            project(0)
             early(load_out[2])
-            project(0)
             prepare(1)
             project(1)
             if opening:

time: 15.8 us -> 15.7 us (level)
  the two profiles are of different devices: /device:TPU:0 before, /device:TPU:17 now
where the time goes in v8:
time: 15.7 us; the launch traced here: 15.5 us
  Pallas kernels  14.8 us (94%)
  local copies, waits for them, and re-layouts  0.62 us (4%)
    pallas_call x1, Pallas kernels, shards(): pl.pallas_call(kernel, out_shape=pltpu.VMEM(tokens_in.shape, tokens_in.dt...  14.8 us
    unnamed x1, local copies, waits for them, and re-layouts  0.62 us

profile of v8, /device:TPU:17, one launch (start us, length us, event | category | flops | bytes accessed | tf_op | source)
XLA Modules:
  0.0 15.5 jit_solution(10185920702703855967)
XLA Ops:
  0.0 14.8 %section_stack.1 = bf16[1,1,8,2048]{3,2,1,0:T(8,128)(2,1)S(1)} custom-call(bf16[1,1,8,2048]{3,2,1,0:T(8,128)(2,1)} %refs_0_.1, bf16[1,2048,512]{2,1,0:T(8,128)(2,1)} %refs_1_.1, f32[1,4,512]{2,1,0:T(4,128)} %refs_2_.1, f32[1,512]{1,0:T(1,128)} %refs_3_.1, bf16[1,8,64,64]{3,2,1,0:T(8,128)(2,1)} %refs_4_.1, f32[1,512]{1,0:T(1,128)} %refs_5_.1, ...), custom_call_target="tpu_custom_call" | custom-call | tf_op jit(solution)/shard_map/section_stack/pallas_call | solution.py:602
  14.8 0.6 %copy.14 = bf16[1,1,8,2048]{3,2,1,0:T(8,128)(2,1)} copy(bf16[1,1,8,2048]{3,2,1,0:T(8,128)(2,1)S(1)} %section_stack.1) | data formatting | bytes 65536

commit v9 on v8

--- a/solution.py
+++ b/solution.py
@@ -80,8 +80,12 @@
     first_stop = leads & (section == 0)
     last_stop = leads & (section == last)
 
+    columns = [column - core + core_index for core_index in range(pair)]
+    onward_stop = jnp.minimum(section + 1, last)
+
     def at(stop, core_index):
-        return {"pp": stop, "tp": column - core + core_index}
+        known = isinstance(core_index, int)
+        return {"pp": stop, "tp": columns[core_index] if known else columns[0] + core_index}
 
     def across(part):
         return slice(part * part_width, (part + 1) * part_width)
@@ -176,7 +180,7 @@
             dst_ref=inbox.at[slot, cores, :, across(part)],
             send_sem=send_sem.at[slot],
             recv_sem=recv_sem.at[slot, first, part],
-            device_id=at(jnp.minimum(section + 1, last), lead),
+            device_id=at(onward_stop, lead),
             device_id_type=MESH,
         )
 
@@ -186,7 +190,7 @@
             dst_ref=inbox.at[slot],
             send_sem=send_sem.at[slot],
             recv_sem=recv_sem.at[slot, 0, 0],
-            device_id=at(jnp.minimum(section + 1, last), lead),
+            device_id=at(onward_stop, lead),
             device_id_type=MESH,
         )
 
@@ -242,7 +246,7 @@
         dst_ref=before,
         send_sem=norm_sem.at[0],
         recv_sem=norm_sem.at[1],
-        device_id=at(jnp.minimum(section + 1, last), lead),
+        device_id=at(onward_stop, lead),
         device_id_type=MESH,
     )
 

time: 15.7 us -> 15.7 us (level)
  no operation moved by 1% of the time
where the time goes in v9:
time: 15.7 us; the launch traced here: 15.5 us
  Pallas kernels  14.8 us (94%)
  local copies, waits for them, and re-layouts  0.62 us (4%)
    pallas_call x1, Pallas kernels, shards(): pl.pallas_call(kernel, out_shape=pltpu.VMEM(tokens_in.shape, tokens_in.dt...  14.8 us
    unnamed x1, local copies, waits for them, and re-layouts  0.62 us

profile of v9, /device:TPU:17, one launch (start us, length us, event | category | flops | bytes accessed | tf_op | source)
XLA Modules:
  0.0 15.5 jit_solution(2435894176845111258)
XLA Ops:
  0.0 14.8 %section_stack.1 = bf16[1,1,8,2048]{3,2,1,0:T(8,128)(2,1)S(1)} custom-call(bf16[1,1,8,2048]{3,2,1,0:T(8,128)(2,1)} %refs_0_.1, bf16[1,2048,512]{2,1,0:T(8,128)(2,1)} %refs_1_.1, f32[1,4,512]{2,1,0:T(4,128)} %refs_2_.1, f32[1,512]{1,0:T(1,128)} %refs_3_.1, bf16[1,8,64,64]{3,2,1,0:T(8,128)(2,1)} %refs_4_.1, f32[1,512]{1,0:T(1,128)} %refs_5_.1, ...), custom_call_target="tpu_custom_call" | custom-call | tf_op jit(solution)/shard_map/section_stack/pallas_call | solution.py:606
  14.8 0.6 %copy.14 = bf16[1,1,8,2048]{3,2,1,0:T(8,128)(2,1)} copy(bf16[1,1,8,2048]{3,2,1,0:T(8,128)(2,1)S(1)} %section_stack.1) | data formatting | bytes 65536
